TPU v7x, 32 devices: a whole 2x2x4 slice. The times are simulated.
32 devices in a mesh: sp: 8 (over z, y), tp: 4 (over x, core).
Axes of the slice: x: 2, y: 2, z: 4, core: 2. Of those that a mesh axis runs over, the one named last changes fastest.
Arguments:
- moe_input: bfloat16 [1024, 2048], P('sp', 'tp'), may hold values from -6 to 6
- cotangent: bfloat16 [1024, 2048], P('sp', 'tp'), may hold values from -6 to 6
- expert_ids: int32 [1024, 2], P('sp'), may hold values from 0 to 7, as said below
- routing_weights: float32 [1024, 2], P('sp'), may hold values from 0.1 to 0.6
- gate_weight: bfloat16 [8, 2048, 1024], P('sp', None, 'tp'), may hold values from -0.125 to 0.125
- up_weight: bfloat16 [8, 2048, 1024], P('sp', None, 'tp'), may hold values from -0.125 to 0.125
- down_weight: bfloat16 [8, 1024, 2048], P('sp', 'tp'), may hold values from -0.1875 to 0.1875
- inner_x: bfloat16 [1024, 4096], P('sp', 'tp'), may hold values from -6 to 6
- inner_b: bfloat16 [1024, 256], P('sp', 'tp'), may hold values from -6 to 6
- inner_c: bfloat16 [1024, 256], P('sp', 'tp'), may hold values from -6 to 6
- gate_z: bfloat16 [1024, 4096], P('sp', 'tp'), may hold values from -6 to 6
- step_raw: float32 [1024, 64], P('sp', 'tp'), may hold values from -30 to 2
- decay_rate: float32 [64], P('tp'), may hold values from 1 to 16
- skip_weight: float32 [64], P('tp'), may hold values from 0.1 to 1.9
- norm_gain: float32 [4096], P('tp'), may hold values from 0.1 to 1.9
- w_out: bfloat16 [2048, 4096], P(None, 'tp'), may hold values from -0.09375 to 0.09375
Outputs:
- gate_weight_gradient: bfloat16 [8, 2048, 1024], P('sp', None, 'tp')
- up_weight_gradient: bfloat16 [8, 2048, 1024], P('sp', None, 'tp')
- down_weight_gradient: bfloat16 [8, 1024, 2048], P('sp', 'tp')
- grad_out: float32 [2048, 4096], P('sp', 'tp')
- grad_inner_x: bfloat16 [1024, 4096], P('sp', 'tp')
- grad_inner_b: float32 [1024, 256], P('sp', 'tp')
- grad_inner_c: float32 [1024, 256], P('sp', 'tp')
- grad_gate_z: bfloat16 [1024, 4096], P('sp', 'tp')
- grad_step_raw: float32 [1024, 64], P('sp', 'tp')
Inputs may be any that keep to these rules, and one draw needn't show every extreme that they name: `expert_ids`: the two entries of a row differ and lie in the same group of 2 consecutive experts. In each aligned block of 128 rows no expert is named more than 64 times; one group of experts, the same for all blocks, takes exactly half of every block's rows, and each of its experts is named exactly 64 times in every block.
All inputs are finite; a program needn't handle non-finite values.
Results may differ from a plain program's by a relative error of at most 0.015.
Values may be sent and summed in bfloat16 or wider, within the bound.
A program may use at most 128 MiB of HBM per device.

v0:
```python
from functools import partial

import jax
import jax.numpy as jnp
from jax import lax
from jax.sharding import PartitionSpec as P

HEAD_DIM = 64
STATE = 64
SPAN = 128


EPS = 0.01
HIGH = lax.Precision.HIGHEST


def carried_in(shard, axis, join, neutral):
    place = lax.axis_index(axis)
    gathered = jax.tree.map(
        lambda a, kind: lax.all_gather(a.astype(kind), axis), shard, (jnp.bfloat16, jnp.bfloat16)
    )
    state = jax.tree.map(lambda a, e: jnp.zeros_like(a) + jnp.asarray(e, a.dtype), shard, neutral)

    def one(step, state):
        return join(
            state,
            jax.tree.map(
                lambda a, own: lax.dynamic_index_in_dim(a, step, 0, False).astype(own.dtype),
                gathered,
                shard,
            ),
        )

    return lax.fori_loop(0, place, one, state)


def carried_in_2(shard, axis, combine, identity):
    devices, mine = (lax.axis_size(axis), lax.axis_index(axis))
    everything = jax.tree.map(
        lambda part, kind: lax.all_gather(part.astype(kind), axis),
        shard,
        jax.tree.map(lambda a: jnp.bfloat16 if a.dtype == jnp.float32 else a.dtype, shard),
    )
    start = jax.tree.map(
        lambda part, zero: jnp.broadcast_to(jnp.asarray(zero, part.dtype), part.shape),
        shard,
        identity,
    )

    def step(k, before):
        at = devices - 1 - k
        reached = at > mine
        new = combine(
            before, jax.tree.map(lambda part, own: part[at].astype(own.dtype), everything, shard)
        )
        return jax.tree.map(lambda a, b: jnp.where(reached, a, b), new, before)

    return lax.fori_loop(0, devices, step, start)


def slot_positions(chosen, expert_list, expert_capacity):
    listed = chosen.reshape(-1)
    onehot = (listed[:, None] == jnp.arange(expert_list, dtype=jnp.int32)[None, :]).astype(
        jnp.int32
    )
    before = jnp.cumsum(onehot, axis=0) - onehot
    return listed * expert_capacity + jnp.sum(before * onehot, axis=1)


def prepare(inner_x32, inner_b32, step_raw, decays):
    tok_rows = inner_x32.shape[0]
    heads = decays.shape[0]
    groups = inner_b32.shape[1] // STATE
    per_group = heads // groups
    blocks = tok_rows // SPAN
    x_act = jax.nn.silu(inner_x32).reshape(tok_rows, heads, HEAD_DIM)
    b_blocks = jax.nn.silu(inner_b32).reshape(blocks, SPAN, groups, STATE)
    step_size = jax.nn.softplus(step_raw)
    decay_log = (-step_size * decays[None, :]).reshape(blocks, SPAN, groups, per_group)
    scaled = (x_act * step_size[:, :, None]).reshape(blocks, SPAN, groups, per_group, HEAD_DIM)
    return (x_act, b_blocks, decay_log, scaled)


def advance(carry_state, block_in):
    x_block, log_block, b_block = block_in
    running = jnp.cumsum(log_block, axis=0)
    to_end = jnp.exp(running[-1] - running)
    fresh_state = jnp.einsum("lgn,lge,lgep->gepn", b_block, to_end, x_block, precision=HIGH)
    return (carry_state * jnp.exp(running[-1])[:, :, None, None] + fresh_state, None)


def block_outputs(carry_state, block_in):
    x_block, log_block, b_block, c_block = block_in
    span_len = x_block.shape[0]
    running = jnp.cumsum(log_block, axis=0)
    places = jnp.arange(span_len)
    causal = (places[:, None] >= places[None, :])[:, :, None, None]
    between = running[:, None] - running[None, :]
    weights = jnp.where(causal, jnp.exp(jnp.where(causal, between, 0.0)), 0.0)
    scores = jnp.einsum("lgn,sgn->lsg", c_block, b_block, precision=HIGH)
    inside = jnp.einsum("lsg,lsge,sgep->lgep", scores, weights, x_block, precision=HIGH)
    carried = jnp.einsum(
        "lgn,gepn,lge->lgep", c_block, carry_state, jnp.exp(running), precision=HIGH
    )
    to_end = jnp.exp(running[-1] - running)
    fresh_state = jnp.einsum("lgn,lge,lgep->gepn", b_block, to_end, x_block, precision=HIGH)
    return (carry_state * jnp.exp(running[-1])[:, :, None, None] + fresh_state, inside + carried)


def mixer_output(
    inner_x32, inner_b32, inner_c32, gate_z32, step_raw, carry_in, decays, skip_weight, norm_gain
):
    tok_rows = inner_x32.shape[0]
    heads = decays.shape[0]
    groups = inner_b32.shape[1] // STATE
    x_act, b_blocks, decay_log, scaled = prepare(inner_x32, inner_b32, step_raw, decays)
    c_blocks = jax.nn.silu(inner_c32).reshape(tok_rows // SPAN, SPAN, groups, STATE)
    outputs = lax.scan(block_outputs, carry_in, (scaled, decay_log, b_blocks, c_blocks))[1]
    mixed_out = outputs.reshape(tok_rows, heads, HEAD_DIM) + x_act * skip_weight[None, :, None]
    gated_out = mixed_out.reshape(tok_rows, heads * HEAD_DIM) * jax.nn.silu(gate_z32)
    grouped = gated_out.reshape(tok_rows, groups, -1)
    normed = grouped * lax.rsqrt(jnp.mean(grouped * grouped, axis=2, keepdims=True) + EPS)
    return normed.reshape(tok_rows, -1) * norm_gain[None, :]


def carry_forward(earlier, latter):
    return (earlier[0] * latter[0], earlier[1] * latter[0][:, :, None, None] + latter[1])


def carry_back(earlier, latter):
    return (latter[0] * earlier[0], latter[1] + latter[0][:, :, None, None] * earlier[1])


def body(
    moe_input,
    cotangent,
    expert_ids,
    routing_weights,
    gate_weight,
    up_weight,
    down_weight,
    inner_x,
    inner_b,
    inner_c,
    gate_z,
    step_raw,
    decay_rate,
    skip_weight,
    norm_gain,
    w_out,
):
    tok_rows, chosen_count = expert_ids.shape
    local_experts = gate_weight.shape[0]
    senders = lax.axis_size("sp")
    expert_list = local_experts * senders
    expert_capacity = 4 * tok_rows // expert_list
    place_into_slots = slot_positions(expert_ids, expert_list, expert_capacity)
    owner = (
        jnp.full((expert_list * expert_capacity,), tok_rows, jnp.int32)
        .at[place_into_slots]
        .set(jnp.arange(tok_rows * chosen_count, dtype=jnp.int32) // chosen_count)
    )
    scaling = (
        jnp.zeros((expert_list * expert_capacity,), jnp.float32)
        .at[place_into_slots]
        .set(routing_weights.reshape(-1))
    )

    def to_slots(source, weighted):
        padded = jnp.concatenate([source, jnp.zeros((1, source.shape[1]), source.dtype)], axis=0)
        picked = padded[owner]
        if weighted:
            picked = (picked.astype(jnp.float32) * scaling[:, None]).astype(jnp.bfloat16)
        return picked.reshape(senders, local_experts, expert_capacity, source.shape[1])

    part_in, part_grad = (
        lax.all_to_all(to_slots(moe_input, False), "sp", split_axis=0, concat_axis=0, tiled=True),
        lax.all_to_all(to_slots(cotangent, True), "sp", split_axis=0, concat_axis=0, tiled=True),
    )
    routed_in, routed_grad = (
        lax.all_gather(part_in, "tp", axis=3, tiled=True),
        lax.all_gather(part_grad, "tp", axis=3, tiled=True),
    )
    gate_pre = jnp.einsum(
        "secd,edf->secf", routed_in, gate_weight, preferred_element_type=jnp.float32
    )
    up_pre = jnp.einsum("secd,edf->secf", routed_in, up_weight, preferred_element_type=jnp.float32)
    sigmoid_gate = jax.nn.sigmoid(gate_pre)
    active = gate_pre * sigmoid_gate
    hidden = (active * up_pre).astype(jnp.bfloat16)
    hidden_grad = jnp.einsum(
        "secd,efd->secf", routed_grad, down_weight, preferred_element_type=jnp.float32
    )
    gate_grad = (
        hidden_grad * up_pre * sigmoid_gate * (1.0 + gate_pre * (1.0 - sigmoid_gate))
    ).astype(jnp.bfloat16)
    up_grad = (hidden_grad * active).astype(jnp.bfloat16)
    slot_terms = jnp.einsum(
        "secf,edf->secd", gate_grad, gate_weight, preferred_element_type=jnp.float32
    )
    slot_terms = slot_terms + jnp.einsum(
        "secf,edf->secd", up_grad, up_weight, preferred_element_type=jnp.float32
    )
    summed = lax.psum_scatter(
        slot_terms.astype(jnp.bfloat16), "tp", scatter_dimension=3, tiled=True
    )
    returned = lax.all_to_all(summed, "sp", split_axis=0, concat_axis=0, tiled=True)
    down_weight_gradient = jnp.einsum(
        "secf,secd->efd", hidden, routed_grad, preferred_element_type=jnp.float32
    ).astype(jnp.bfloat16)
    gate_weight_gradient = jnp.einsum(
        "secd,secf->edf", routed_in, gate_grad, preferred_element_type=jnp.float32
    ).astype(jnp.bfloat16)
    up_weight_gradient = jnp.einsum(
        "secd,secf->edf", routed_in, up_grad, preferred_element_type=jnp.float32
    ).astype(jnp.bfloat16)
    back_rows = returned.reshape(expert_list * expert_capacity, returned.shape[3])
    moe_grad = jnp.sum(
        back_rows[place_into_slots].astype(jnp.float32).reshape(tok_rows, chosen_count, -1), axis=1
    )
    mixer_cols = (cotangent.astype(jnp.float32) + moe_grad).astype(jnp.bfloat16)
    mixer_rows = lax.all_gather(mixer_cols, "tp", axis=1, tiled=True)
    inner_x32 = inner_x.astype(jnp.float32)
    inner_b32 = inner_b.astype(jnp.float32)

    def local_states(x_in, b_in, raw_in):
        x_act, b_blocks, decay_log, scaled = prepare(x_in, b_in, raw_in, decay_rate)
        totals = jnp.exp(jnp.sum(decay_log, axis=(0, 1)))
        initial = jnp.zeros((decay_log.shape[2], decay_log.shape[3], HEAD_DIM, STATE), jnp.float32)
        return (totals, lax.scan(advance, initial, (scaled, decay_log, b_blocks))[0])

    (totals, fresh), states_pull = jax.vjp(local_states, inner_x32, inner_b32, step_raw)
    identity = (jnp.ones_like(totals), jnp.zeros_like(fresh))
    carry_in = carried_in((totals, fresh), "sp", carry_forward, identity)[1]
    output_fn = partial(
        mixer_output, decays=decay_rate, skip_weight=skip_weight, norm_gain=norm_gain
    )
    normed, output_pull = jax.vjp(
        output_fn,
        inner_x32,
        inner_b32,
        inner_c.astype(jnp.float32),
        gate_z.astype(jnp.float32),
        step_raw,
        carry_in,
    )
    norm_rows = normed.astype(jnp.bfloat16)
    grad_out = lax.psum_scatter(
        lax.dot_general(
            mixer_rows, norm_rows, (((0,), (0,)), ((), ())), preferred_element_type=jnp.float32
        ),
        "sp",
        scatter_dimension=0,
        tiled=True,
    )
    norm_grad = jnp.dot(mixer_rows, w_out, preferred_element_type=jnp.float32)
    x_grad_out, b_grad_out, c_grad, z_grad, raw_grad_out, state_grad = output_pull(norm_grad)
    after_grad = carried_in_2((totals, state_grad), "sp", carry_back, identity)[1]
    x_grad_state, b_grad_state, raw_grad_state = states_pull(
        (jnp.sum(after_grad * carry_in, axis=(2, 3)), after_grad)
    )
    grad_inner_x = (x_grad_out + x_grad_state).astype(jnp.bfloat16)
    grad_inner_b = b_grad_out + b_grad_state
    grad_step_raw = raw_grad_out + raw_grad_state
    return (
        gate_weight_gradient,
        up_weight_gradient,
        down_weight_gradient,
        grad_out,
        grad_inner_x,
        grad_inner_b,
        c_grad,
        z_grad.astype(jnp.bfloat16),
        grad_step_raw,
    )


def solution(mesh):
    return jax.shard_map(
        body,
        mesh=mesh,
        in_specs=(
            P("sp", "tp"),
            P("sp", "tp"),
            P("sp", None),
            P("sp", None),
            P("sp", None, "tp"),
            P("sp", None, "tp"),
            P("sp", "tp", None),
            P("sp", "tp"),
            P("sp", "tp"),
            P("sp", "tp"),
            P("sp", "tp"),
            P("sp", "tp"),
            P("tp"),
            P("tp"),
            P("tp"),
            P(None, "tp"),
        ),
        out_specs=(
            P("sp", None, "tp"),
            P("sp", None, "tp"),
            P("sp", "tp", None),
            P("sp", "tp"),
            P("sp", "tp"),
            P("sp", "tp"),
            P("sp", "tp"),
            P("sp", "tp"),
            P("sp", "tp"),
        ),
        check_vma=False,
    )
```

profile of v0, /device:TPU:0, one launch (start us, length us, event | category | flops | bytes accessed | tf_op | source)
XLA Modules:
  0.0 389.4 jit_solution(15698069965374357368)
XLA Ops:
  13.5 2.0 gather_fusion
  15.5 21.7 %all_to_all.15 = bf16[8,1,64,512]{3,2,1,0:T(8,128)(2,1)} all-to-all(bf16[8,1,64,512]{3,2,1,0:T(8,128)(2,1)S(1)} %bitcast.348), channel_id=1, replica_groups=mesh['sp'=8,'tp'=4] {'sp'}, dimensions={0} | all-to-all | bytes 1048576 | tf_op jit(solution)/shard_map/all_to_all | solution.py:177
  39.1 2.0 gather_fusion.1
  41.2 17.6 %all_to_all.16 = bf16[8,1,64,512]{3,2,1,0:T(8,128)(2,1)} all-to-all(bf16[8,1,64,512]{3,2,1,0:T(8,128)(2,1)S(1)} %fusion.32), channel_id=1, replica_groups=mesh['sp'=8,'tp'=4] {'sp'}, dimensions={0} | all-to-all | bytes 1048576 | tf_op jit(solution)/shard_map/all_to_all | solution.py:178
  59.0 2.5 fusion.20
  62.2 20.9 %all-gather.10.cloned.1.call-done = bf16[8,1,64,2048]{3,2,0,1:T(8,128)(2,1)} async-done(((bf16[8,1,64,512]{3,2,0,1:T(8,128)(2,1)}), bf16[8,1,64,2048]{3,2,0,1:T(8,128)(2,1)}) %all-gather.10.cloned.1.call-update) | async-done | bytes 2097168 | tf_op jit(solution)/shard_map/all_gather | solution.py:182
  83.1 2.7 fusion.88
  86.6 2.1 fusion.1
  94.6 21.8 %all-reduce.6 = bf16[128]{0:T(256)(128)(2,1)S(1)} all-reduce(bf16[128]{0:T(256)(128)(2,1)S(1)} %dynamic-update-slice), channel_id=2, replica_groups=mesh['sp'=8,'tp'=4] {'sp'}, use_global_device_ids=true, to_apply=%add.6 | all-reduce | flops 128 | bytes 512
  117.1 2.9 reduce-scatter.3.cloned.1.call-done
  120.1 5.5 %all-to-all-start.2 = ((bf16[8,1,64,512]{3,2,1,0:T(8,128)(2,1)}), bf16[8,1,64,512]{3,2,1,0:T(8,128)(2,1)S(1)}, u32[]{:S(2)}, u32[]{:S(2)}) async-start(bf16[8,1,64,512]{3,2,1,0:T(8,128)(2,1)} %bitcast.359), calls=%async_computation.3 | async-start | bytes 1048576 | tf_op jit(solution)/shard_map/all_to_all | solution.py:207
  125.7 24.6 %all-gather.12.cloned.1.call-done = bf16[128,64,64]{2,1,0:T(8,128)(2,1)} async-done(((bf16[16,64,64]{2,1,0:T(8,128)(2,1)}), bf16[128,64,64]{2,1,0:T(8,128)(2,1)}) %all-gather.12.cloned.1.call-update) | async-done | bytes 1048592 | tf_op jit(solution)/shard_map/all_gather | solution.py:20
  152.0 3.1 fusion.27
  156.3 2.0 gather_fusion.2
  162.0 7.1 %all_gather.29 = bf16[128,2048]{1,0:T(8,128)(2,1)S(1)} all-gather(bf16[128,512]{1,0:T(8,128)(2,1)S(1)} %add_convert_fusion.1), channel_id=1, replica_groups=mesh['sp'=8,'tp'=4] {'tp'}, dimensions={1}, use_global_device_ids=true | all-gather | bytes 655360 | tf_op jit(solution)/shard_map/all_gather | solution.py:222
  169.1 3.5 multiply_reduce_fusion.8
  174.2 2.0 fusion.29
  176.5 5.7 %fusion.91 = f32[2048,1024]{1,0:T(8,128)} fusion(bf16[128,2048]{1,0:T(8,128)(2,1)} %copy-done.3, f32[128,1024]{1,0:T(8,128)} %copy-done.9, f32[1024]{0:T(1024)} %param.35, f32[128]{0:T(128)} %copy-done.31), kind=kOutput, calls=%fused_computation.141 | convolution fusion | flops 537264128 | bytes 9441792 | tf_op jit(solution)/shard_map/dot_general | solution.py:249
  185.8 2.1 copy.126
  187.8 2.1 convolution_bitcast_fusion.6
  191.1 3.5 fusion.6
  194.6 1.7 fusion.7
  196.8 1.8 fusion.5
  200.6 3.9 %fusion.44 = (f32[128,16]{0,1:T(8,128)}, f32[128,16]{0,1:T(8,128)}, f32[128,128]{1,0:T(8,128)}) fusion(f32[128,16]{0,1:T(8,128)} %copy-done.30, f32[128,128]{1,0:T(8,128)} %copy-done.25, pred[128,128]{1,0:T(8,128)(4,1)} %copy-done.29, f32[16,128,64]{1,2,0:T(8,128)S(1)} %bitcast.344, f32[128,16,64]{0,2,1:T(8,128)S(1)} %bitcast.341, f32[128,16]{0,1:T(8,128)S(1)} %copy.117), kind=kOutput, calls=%fused_computation.78 | convolution fusion | flops 204320768 | bytes 1228800 | tf_op jit(solution)/shard_map/transpose(jvp())/while/body/eval_jaxpr/lsg,lsge,sgep->lgep/dot_general | solution.py:101
  205.9 1.4 copy.138
  207.3 3.2 fusion.26
  210.6 2.1 copy.125
  212.6 1.7 fusion.31
  214.3 1.7 convolution_bitcast_fusion.10
  216.0 1.7 fusion.122
  217.7 14.2 %all-gather.14.cloned.1.call-done = bf16[128,64,64]{2,1,0:T(8,128)(2,1)} async-done(((bf16[16,64,64]{2,1,0:T(8,128)(2,1)}), bf16[128,64,64]{2,1,0:T(8,128)(2,1)}) %all-gather.14.cloned.1.call-update) | async-done | bytes 1048592 | tf_op jit(solution)/shard_map/all_gather | solution.py:40
  231.9 14.3 %while.22 = (s32[]{:T(128)}, f32[1,16,64,64]{3,2,1,0:T(8,128)S(1)}, s32[]{:T(128)}, bf16[8,1,16,64,64]{4,3,2,1,0:T(8,128)(2,1)}, bf16[8,1,16]{2,1,0:T(2,128)(2,1...) while((s32[]{:T(128)}, f32[1,16,64,64]{3,2,1,0:T(8,128)S(1)}, s32[]{:T(128)}, ...), condition=%wide.region_15.17_spmd.clone, body=%wide.region_14.16_spmd.clone.sunk | while | flops 327704 | bytes 655695 | solution.py:58
  246.2 3.2 multiply_reduce_fusion.1
  249.4 1.4 copy.167
  250.8 1.4 copy.156
  253.1 2.1 multiply_reduce_fusion.11
  255.2 1.6 fusion.114
  256.8 2.0 reduce_window_sum.62
  259.5 1.5 pad_add_fusion
  261.0 2.0 reduce_window_sum.64
  262.9 1.4 copy.140
  264.3 1.4 copy.139
  266.4 1.6 fusion.113
  268.1 1.5 copy.144
  269.6 2.1 copy.130
  271.7 2.4 fusion.128
  274.1 2.4 fusion.57
  276.5 105.6 %reduce-scatter.5.cloned.1.call-done = f32[256,1024]{1,0:T(8,128)} async-done(((f32[2048,1024]{1,0:T(8,128)}), f32[256,1024]{1,0:T(8,128)}) %reduce-scatter.5.cloned.1.call-update) | async-done | bytes 1048592 | tf_op jit(solution)/shard_map/reduce_scatter | solution.py:248
  (184 shorter events, 48.0 us)
Async XLA Ops:
  8.0 51.0 %copy-start = (bf16[1,2048,256]{2,1,0:T(8,128)(2,1)S(1)}, bf16[1,2048,256]{2,1,0:T(8,128)(2,1)}, u32[]{:S(2)}) copy-start(bf16[1,2048,256]{2,1,0:T(8,128)(2,1)} %param.25) | copy-start | bytes 3145732
  8.0 50.9 %all-gather.8.cloned.1.call-start = ((), (), s32[]{:S(2)}) async-start(), calls=%async_computation.5 | async-start | bytes 2621440 | tf_op jit(solution)/shard_map/all_gather | solution.py:181
  13.5 23.8 %copy-start.35 = (f32[128,2]{0,1:T(2,128)S(1)}, f32[128,2]{0,1:T(2,128)}, u32[]{:S(2)}) copy-start(f32[128,2]{0,1:T(2,128)} %param.24) | copy-start | bytes 3076
  13.5 25.6 %copy-start.13 = (bf16[128,512]{1,0:T(8,128)(2,1)S(1)}, bf16[128,512]{1,0:T(8,128)(2,1)}, u32[]{:S(2)}) copy-start(bf16[128,512]{1,0:T(8,128)(2,1)} %param.22) | copy-start | bytes 393220
  37.2 45.9 %all-gather.10.cloned.1.call-start = ((), (), s32[]{:S(2)}) async-start(), calls=%async_computation.6 | async-start | bytes 2621440 | tf_op jit(solution)/shard_map/all_gather | solution.py:182
  58.8 2.6 copy-start.11
  58.9 61.2 %reduce-scatter.3.cloned.1.call-start = ((), (), s32[]{:S(2)}) async-start(), calls=%async_computation.7 | async-start | bytes 2621440 | tf_op jit(solution)/shard_map/reduce_scatter | solution.py:204
  59.0 2.5 copy-start.38
  61.5 24.3 %copy-start.14 = (f32[8,1,64,256]{3,2,0,1:T(8,128)}, f32[8,1,64,256]{3,2,0,1:T(8,128)S(1)}, u32[]{:S(2)}) copy-start(f32[8,1,64,256]{3,2,0,1:T(8,128)S(1)} %fusion.20) | copy-start | bytes 1572868
  62.2 23.6 %copy-start.16 = (f32[8,1,64,256]{3,2,0,1:T(8,128)}, f32[8,1,64,256]{3,2,0,1:T(8,128)S(1)}, u32[]{:S(2)}) copy-start(f32[8,1,64,256]{3,2,0,1:T(8,128)S(1)} %fusion.17) | copy-start | bytes 1572868
  85.8 0.8 copy-start.20
  85.8 0.8 copy-start.22
  88.7 0.7 copy-start.28
  88.7 0.8 copy-start.33
  88.7 1.4 copy-start.4
  88.7 1.8 copy-start.18
  88.8 3.1 copy-start.37
  88.8 3.9 copy-start.24
  88.8 4.3 %copy-start.40 = (u32[32]{0:T(128)S(1)}, u32[32]{0:T(128)}, u32[]{:S(2)}) copy-start(u32[32]{0:T(128)} %constant.265) | copy-start | bytes 388
  88.8 61.5 %all-gather.12.cloned.1.call-start = ((), (), s32[]{:S(2)}) async-start(), calls=%async_computation.9 | async-start | bytes 2359296 | tf_op jit(solution)/shard_map/all_gather | solution.py:20
  89.5 0.6 copy-start.12
  89.6 30.5 %copy-start.36 = (f32[16]{0:T(128)}, f32[16]{0:T(128)S(1)}, u32[]{:S(2)}) copy-start(f32[16]{0:T(128)S(1)} %get-tuple-element.613) | copy-start | bytes 196
  90.5 2.2 copy-start.34
  91.9 59.3 %copy-start.30 = (f32[128,16]{0,1:T(8,128)}, f32[128,16]{0,1:T(8,128)S(1)}, u32[]{:S(2)}) copy-start(f32[128,16]{0,1:T(8,128)S(1)} %copy.114) | copy-start | bytes 24580
  93.1 58.1 %copy-start.25 = (f32[128,128]{1,0:T(8,128)}, f32[128,128]{1,0:T(8,128)S(1)}, u32[]{:S(2)}) copy-start(f32[128,128]{1,0:T(8,128)S(1)} %copy.107) | copy-start | bytes 196612
  116.5 34.7 %copy-start.23 = (f32[128,16]{0,1:T(8,128)}, f32[128,16]{0,1:T(8,128)S(1)}, u32[]{:S(2)}) copy-start(f32[128,16]{0,1:T(8,128)S(1)} %copy.118) | copy-start | bytes 24580
  117.1 34.0 %copy-start.29 = (pred[128,128]{1,0:T(8,128)(4,1)}, pred[128,128]{1,0:T(8,128)(4,1)S(1)}, u32[]{:S(2)}) copy-start(pred[128,128]{1,0:T(8,128)(4,1)S(1)} %iota_compare_fusion) | copy-start | bytes 49156
  120.1 36.2 %all-to-all-start.2 = ((bf16[8,1,64,512]{3,2,1,0:T(8,128)(2,1)}), bf16[8,1,64,512]{3,2,1,0:T(8,128)(2,1)S(1)}, u32[]{:S(2)}, u32[]{:S(2)}) async-start(bf16[8,1,64,512]{3,2,1,0:T(8,128)(2,1)} %bitcast.359), calls=%async_computation.3 | async-start | bytes 1048576 | tf_op jit(solution)/shard_map/all_to_all | solution.py:207
  125.6 106.3 %all-gather.14.cloned.1.call-start = ((), (), s32[]{:S(2)}) async-start(), calls=%async_computation.10 | async-start | bytes 2359296 | tf_op jit(solution)/shard_map/all_gather | solution.py:40
  150.5 4.5 %copy-start.32 = (bf16[8,1,16]{2,1,0:T(2,128)(2,1)}, bf16[8,1,16]{2,1,0:T(2,128)(2,1)S(1)}, u32[]{:S(2)}) copy-start(bf16[8,1,16]{2,1,0:T(2,128)(2,1)S(1)} %get-tuple-element.766) | copy-start | bytes 772
  151.2 0.8 copy-start.7
  169.1 3.6 copy-start.3
  169.1 3.6 copy-start.19
  169.1 3.6 copy-start.26
  172.7 1.3 copy-start.9
  172.7 1.3 copy-start.31
  174.0 8.3 %copy-start.1 = (f32[128,1024]{1,0:T(8,128)}, f32[128,1024]{1,0:T(8,128)S(1)}, u32[]{:S(2)}) copy-start(f32[128,1024]{1,0:T(8,128)S(1)} %get-tuple-element.616) | copy-start | bytes 1572868
  176.2 205.9 %reduce-scatter.5.cloned.1.call-start = ((), (), s32[]{:S(2)}) async-start(), calls=%async_computation.8 | async-start | bytes 9437184 | tf_op jit(solution)/shard_map/reduce_scatter | solution.py:248
  191.1 3.5 copy-start.21
  191.1 3.5 copy-start.39
  194.6 1.8 copy-start.6
  194.6 1.8 copy-start.15
  194.6 2.2 copy-start.17
  196.8 1.8 copy-start.8
  231.9 14.3 %copy-start.10 = (f32[128,16,64]{0,2,1:T(8,128)S(1)}, f32[128,16,64]{0,2,1:T(8,128)}, u32[]{:S(2)}) copy-start(f32[128,16,64]{0,2,1:T(8,128)} %convolution_bitcast_fusion.6) | copy-start | bytes 1572868
  253.1 21.0 %copy-start.2 = (f32[128,1024]{1,0:T(8,128)S(1)}, f32[128,1024]{1,0:T(8,128)}, u32[]{:S(2)}) copy-start(f32[128,1024]{1,0:T(8,128)} %copy-done.1) | copy-start | bytes 1572868
  253.1 21.0 %copy-start.5 = (f32[128,1024]{1,0:T(8,128)S(1)}, f32[128,1024]{1,0:T(8,128)}, u32[]{:S(2)}) copy-start(f32[128,1024]{1,0:T(8,128)} %copy.126) | copy-start | bytes 1572868
  268.1 6.0 %copy-start.27 = (f32[1024]{0:T(1024)S(1)}, f32[1024]{0:T(1024)}, u32[]{:S(2)}) copy-start(f32[1024]{0:T(1024)} %mul.488) | copy-start | bytes 12292
Sparse Core Ops, SparseCore 0:
  37.4 21.5 all-gather.7
  60.5 22.5 all-gather.9
  88.9 31.1 reduce-scatter.2
Sparse Core Ops, SparseCore 1:
  92.0 58.3 all-gather.11
  176.3 55.6 all-gather.13
  236.0 146.0 reduce-scatter.4
where the time goes:
time: 392 us; the launch traced here: 389 us
  waiting for transfers between devices  168 us (43%)
  blocking collectives  68.3 us (17%)
  matrix products  53.3 us (14%)
  local copies, waits for them, and re-layouts  38.6 us (10%)
  other arithmetic  37.7 us (10%)
  between operations  16.7 us (4%)
  starting transfers between devices  5.99 us (2%)
    reduce_scatter x1, waiting for transfers between devices, body(): lax.psum_scatter(lax.dot_general(mixer_rows, norm_rows, (((0,), (0,)), ((...  106 us
    all_gather x1, waiting for transfers between devices, carried_in(): lax.all_gather(a.astype(kind), axis)  24.6 us
    unnamed x1, blocking collectives  21.8 us
    all_to_all x1, blocking collectives, body(): lax.all_to_all(to_slots(moe_input, False), 'sp', split_axis=0, concat_axi...  21.7 us
    all_gather x1, waiting for transfers between devices, body(): lax.all_gather(part_grad, 'tp', axis=3, tiled=True)  20.9 us
    all_to_all x1, blocking collectives, body(): lax.all_to_all(to_slots(cotangent, True), 'sp', split_axis=0, concat_axis...  17.6 us
    all_gather x1, waiting for transfers between devices, carried_in_2(): lax.all_gather(part.astype(kind), axis)  14.2 us
    dot_general x3, matrix products, block_outputs(): jnp.einsum('lsg,lsge,sgep->lgep', scores, weights, x_block, precision=HIGH)  10.2 us
  transfers between devices with their start and end apart: 7, of which 5 were waited for; matrix products, arithmetic and copies ran while one was open for 26% of the time, Pallas kernels for 0%

commit v1 on v0

v1 whole, which is shorter than its diff:
```python
from functools import partial

import jax
import jax.numpy as jnp
from jax import lax
from jax.experimental import pallas as pl
from jax.experimental.pallas import tpu as pltpu
from jax.sharding import PartitionSpec as P

HEAD_DIM = 64
STATE = 64
PAIR = 2 * HEAD_DIM
EPS = 0.01
HIGH = lax.Precision.HIGHEST
F32 = jnp.float32
BF16 = jnp.bfloat16


def call(kernel, outs, flops, scratch=()):
    return pl.pallas_call(
        kernel,
        out_shape=[jax.ShapeDtypeStruct(s, d) for s, d in outs],
        scratch_shapes=list(scratch),
        cost_estimate=pl.CostEstimate(flops=flops, bytes_accessed=4_000_000, transcendentals=0),
        compiler_params=pltpu.CompilerParams(vmem_limit_bytes=48 * 1024 * 1024),
    )


def nn(a, b):
    return jnp.dot(a.astype(BF16), b.astype(BF16), preferred_element_type=F32)


def tn(a, b):
    return lax.dot_general(
        a.astype(BF16), b.astype(BF16), (((0,), (0,)), ((), ())), preferred_element_type=F32
    )


def nt(a, b):
    return lax.dot_general(
        a.astype(BF16), b.astype(BF16), (((1,), (1,)), ((), ())), preferred_element_type=F32
    )


def spread(heads):
    rows = lax.broadcasted_iota(jnp.int32, (heads, heads * HEAD_DIM), 0)
    cols = lax.broadcasted_iota(jnp.int32, (heads, heads * HEAD_DIM), 1)
    return (cols // HEAD_DIM == rows).astype(F32)


def wide(v, table):
    return jnp.dot(v, table, precision=HIGH, preferred_element_type=F32)


def narrow(v, table):
    return lax.dot_general(
        v, table, (((1,), (1,)), ((), ())), precision=HIGH, preferred_element_type=F32
    )


def silu_and_slope(v):
    s = jax.nn.sigmoid(v)
    return v * s, s * (1.0 + v * (1.0 - s))


def silu(v):
    return v * jax.nn.sigmoid(v)


def causal_of(rows):
    return lax.broadcasted_iota(jnp.int32, (rows, rows), 0) >= lax.broadcasted_iota(
        jnp.int32, (rows, rows), 1
    )


def decay_table(causal, run_ref, run_t_ref, head):
    gap = run_ref[:, head : head + 1] - run_t_ref[head : head + 1, :]
    return jnp.where(causal, jnp.exp(jnp.where(causal, gap, 0.0)), 0.0)


def fresh_kernel(x_ref, b_ref, dt_ref, run_ref, fresh_ref):
    table = spread(dt_ref.shape[1])
    run = run_ref[...]
    factor = dt_ref[...] * jnp.exp(run[-1:, :] - run)
    xe = silu(x_ref[...].astype(F32)) * wide(factor, table)
    fresh_ref[...] = tn(silu(b_ref[...].astype(F32)), xe).astype(BF16)


def weighted_sum(all_ref, weight_ref):
    def one(j, total):
        return total + all_ref[j].astype(F32) * weight_ref[pl.ds(j, 1), :]

    return lax.fori_loop(0, all_ref.shape[0], one, jnp.zeros(all_ref.shape[1:], F32))


def forward_kernel(
    x_ref, b_ref, c_ref, z_ref, dt_ref, run_ref, run_t_ref, skip_ref, gain_ref, all_ref, coef_ref,
    norm_ref, mixed_ref, state_ref, weight_ref,
):
    heads = dt_ref.shape[1]
    table = spread(heads)
    weight_ref[...] = wide(coef_ref[...], table)
    state = weighted_sum(all_ref, weight_ref)
    state_ref[...] = state
    x_act = silu(x_ref[...].astype(F32))
    xs = (x_act * wide(dt_ref[...], table)).astype(BF16)
    b_act = silu(b_ref[...].astype(F32))
    c_act = silu(c_ref[...].astype(F32))
    mixed_ref[...] = nn(c_act, state) * wide(jnp.exp(run_ref[...]), table) + x_act * wide(
        skip_ref[...], table
    )
    rows = x_ref.shape[0]
    causal = causal_of(rows)
    scores = nt(c_act, b_act)
    first = lax.broadcasted_iota(jnp.int32, (rows, PAIR), 1) < HEAD_DIM
    for pair in range(heads // 2):
        lo = pair * PAIR
        part = xs[:, lo : lo + PAIR]
        one = nn(scores * decay_table(causal, run_ref, run_t_ref, 2 * pair), part)
        two = nn(scores * decay_table(causal, run_ref, run_t_ref, 2 * pair + 1), part)
        mixed_ref[:, lo : lo + PAIR] += jnp.where(first, one, two)
    gated = mixed_ref[...] * silu(z_ref[...].astype(F32))
    scale = lax.rsqrt(jnp.mean(gated * gated, axis=1, keepdims=True) + EPS)
    norm_ref[...] = (gated * scale * gain_ref[...]).astype(BF16)


def backward_kernel(
    x_ref, b_ref, c_ref, z_ref, dt_ref, run_ref, run_t_ref, skip_ref, gain_ref, mixed_ref,
    state_ref, up_ref,
    state_grad_ref, xs_grad_ref, x_grad_ref, z_grad_ref, run_grad_ref, b_grad_ref, c_grad_ref,
):
    heads = dt_ref.shape[1]
    rows = x_ref.shape[0]
    table = spread(heads)
    z_act, z_slope = silu_and_slope(z_ref[...].astype(F32))
    mixed = mixed_ref[...]
    gated = mixed * z_act
    scale = lax.rsqrt(jnp.mean(gated * gated, axis=1, keepdims=True) + EPS)
    up = up_ref[...] * gain_ref[...]
    inner = jnp.mean(up * gated, axis=1, keepdims=True)
    gated_grad = scale * (up - gated * (scale * scale * inner))
    z_grad_ref[...] = (gated_grad * mixed * z_slope).astype(BF16)
    dy = gated_grad * z_act
    x_act = silu(x_ref[...].astype(F32))
    x_grad_ref[...] = dy * wide(skip_ref[...], table)
    xs = (x_act * wide(dt_ref[...], table)).astype(BF16)
    b_act = silu(b_ref[...].astype(F32))
    c_act, c_slope = silu_and_slope(c_ref[...].astype(F32))
    state = state_ref[...]
    grown = dy * wide(jnp.exp(run_ref[...]), table)
    state_grad_ref[...] = tn(c_act, grown).astype(BF16)
    c_grad = nt(grown, state)
    run_grad = narrow(grown * nn(c_act, state), table)
    causal = causal_of(rows)
    scores = nt(c_act, b_act)
    scores_grad = jnp.zeros((rows, rows), F32)
    first = lax.broadcasted_iota(jnp.int32, (rows, PAIR), 1) < HEAD_DIM
    lane = lax.broadcasted_iota(jnp.int32, (rows, heads), 1)
    for pair in range(heads // 2):
        lo = pair * PAIR
        part = xs[:, lo : lo + PAIR]
        dy_part = dy[:, lo : lo + PAIR]
        got = []
        for k in range(2):
            head = 2 * pair + k
            decay = decay_table(causal, run_ref, run_t_ref, head)
            weights = scores * decay
            mine = jnp.where(first if k == 0 else ~first, dy_part, 0.0)
            got.append(tn(weights, mine))
            weights_grad = nt(mine, part)
            scores_grad += weights_grad * decay
            flow = weights_grad * weights
            change = jnp.sum(flow - flow.T, axis=1, keepdims=True)
            run_grad += jnp.where(lane == head, change, 0.0)
        xs_grad_ref[:, lo : lo + PAIR] = got[0] + got[1]
    run_grad_ref[...] = run_grad
    b_grad_ref[...] = tn(scores_grad, c_act)
    c_grad_ref[...] = (c_grad + nn(scores_grad, b_act)) * c_slope


def finish_kernel(
    x_ref, b_ref, raw_ref, dt_ref, run_ref, rate_ref, state_ref, all_ref, coef_ref, xs_grad_ref,
    x_grad_ref, run_grad_ref, b_grad_ref,
    x_out_ref, b_out_ref, raw_out_ref, weight_ref,
):
    heads = dt_ref.shape[1]
    rows = x_ref.shape[0]
    table = spread(heads)
    weight_ref[...] = wide(coef_ref[...], table)
    after = weighted_sum(all_ref, weight_ref)
    x_act, x_slope = silu_and_slope(x_ref[...].astype(F32))
    b_act, b_slope = silu_and_slope(b_ref[...].astype(F32))
    dt = dt_ref[...]
    dt_wide = wide(dt, table)
    run = run_ref[...]
    last = run[-1:, :]
    to_end = wide(jnp.exp(last - run), table)
    moved = nn(b_act, after) * to_end
    xs = x_act * dt_wide
    xs_grad = xs_grad_ref[...] + moved
    b_grad = b_grad_ref[...] + nt(xs * to_end, after)
    out_flow = narrow(xs * moved, table)
    whole = jnp.exp(last) * narrow(
        jnp.sum(after * state_ref[...], axis=0, keepdims=True), table
    )
    at_end = jnp.sum(out_flow, axis=0, keepdims=True) + whole
    run_grad = run_grad_ref[...] - out_flow
    causal = causal_of(rows).astype(F32)
    log_grad = at_end + lax.dot_general(
        causal, run_grad, (((0,), (0,)), ((), ())), precision=HIGH, preferred_element_type=F32
    )
    dt_grad = narrow(x_act * xs_grad, table) - rate_ref[...] * log_grad
    raw_out_ref[...] = dt_grad * jax.nn.sigmoid(raw_ref[...])
    b_out_ref[...] = b_grad * b_slope
    x_out_ref[...] = ((x_grad_ref[...] + xs_grad * dt_wide) * x_slope).astype(BF16)


def picks(ids, slots, experts):
    rows = ids.shape[0]
    capacity = slots // experts
    choice = lax.broadcasted_iota(jnp.int32, (rows, experts), 1)
    hot = [(ids[:, k : k + 1] == choice).astype(F32) for k in range(ids.shape[1])]
    strict = (
        lax.broadcasted_iota(jnp.int32, (rows, rows), 0)
        > lax.broadcasted_iota(jnp.int32, (rows, rows), 1)
    ).astype(F32)
    before = nn(strict, sum(hot))
    place = lax.broadcasted_iota(jnp.int32, (rows, slots), 1)
    found = []
    for k, one in enumerate(hot):
        rank = jnp.sum(before * one, axis=1, keepdims=True).astype(jnp.int32)
        found.append((place == ids[:, k : k + 1] * capacity + rank).astype(BF16))
    return found


def dispatch_kernel(experts, x_ref, cot_ref, ids_ref, weight_ref, out_ref):
    slots = out_ref.shape[0]
    cols = x_ref.shape[1]
    found = picks(ids_ref[...], slots, experts)
    cot = cot_ref[...].astype(F32)
    total = jnp.zeros((slots, cols), F32)
    for k, one in enumerate(found):
        total += tn(one, (cot * weight_ref[:, k : k + 1]).astype(BF16))
    out_ref[:, :cols] = tn(sum(found), x_ref[...]).astype(BF16)
    out_ref[:, cols:] = total.astype(BF16)


def combine_kernel(experts, back_ref, cot_ref, ids_ref, out_ref):
    found = picks(ids_ref[...], back_ref.shape[0], experts)
    moe_grad = nn(sum(found), back_ref[...])
    out_ref[...] = (cot_ref[...].astype(F32) + moe_grad).astype(BF16)


def carries(last, axis):
    count, me = lax.axis_size(axis), lax.axis_index(axis)
    ends = lax.all_gather(last, axis)
    j = jnp.arange(count)
    i = j[None, :]
    ahead = ((i > j[:, None]) & (i < me)).astype(F32)
    behind = ((i < j[:, None]) & (i > me)).astype(F32)
    fore = jnp.where((j < me)[:, None], jnp.exp(jnp.dot(ahead, ends, precision=HIGH)), 0.0)
    back = jnp.where((j > me)[:, None], jnp.exp(jnp.dot(behind, ends, precision=HIGH)), 0.0)
    return fore, back


def body(
    moe_input, cotangent, expert_ids, routing_weights, gate_weight, up_weight, down_weight,
    inner_x, inner_b, inner_c, gate_z, step_raw, decay_rate, skip_weight, norm_gain, w_out,
):
    rows, chosen = expert_ids.shape
    senders = lax.axis_size("sp")
    experts = gate_weight.shape[0] * senders
    capacity = 4 * rows // experts
    slots = experts * capacity
    cols = moe_input.shape[1]
    heads = decay_rate.shape[0]
    inner = heads * HEAD_DIM
    rate, skip, gain = decay_rate[None, :], skip_weight[None, :], norm_gain[None, :]

    dt = jax.nn.softplus(step_raw)
    run = jnp.cumsum(-dt * rate, axis=0)
    run_t = run.T
    (fresh,) = call(fresh_kernel, [((STATE, inner), BF16)], 40_000_000)(inner_x, inner_b, dt, run)
    fresh_all = lax.all_gather(fresh, "sp")
    fore, back = carries(run[-1], "sp")

    (sent,) = call(partial(dispatch_kernel, experts), [((slots, 2 * cols), BF16)], 200_000_000)(
        moe_input, cotangent, expert_ids, routing_weights
    )
    routed = lax.all_to_all(
        sent.reshape(senders, slots // senders, 2 * cols), "sp", 0, 0, tiled=True
    ).reshape(slots, 2 * cols)
    routed = lax.all_gather(routed, "tp")

    weight_rows = pltpu.VMEM((senders, inner), F32)
    norm_rows, mixed, state = call(
        forward_kernel,
        [((rows, inner), BF16), ((rows, inner), F32), ((STATE, inner), F32)],
        300_000_000,
        [weight_rows],
    )(inner_x, inner_b, inner_c, gate_z, dt, run, run_t, skip, gain, fresh_all, fore)
    norm_all = lax.all_gather(norm_rows, "sp", axis=0, tiled=True)

    routed_in = jnp.concatenate([routed[k, :, :cols] for k in range(routed.shape[0])], axis=1)
    routed_grad = jnp.concatenate([routed[k, :, cols:] for k in range(routed.shape[0])], axis=1)
    gate_w, up_w, down_w = gate_weight[0], up_weight[0], down_weight[0]
    gate_pre = jnp.dot(routed_in, gate_w, preferred_element_type=F32)
    up_pre = jnp.dot(routed_in, up_w, preferred_element_type=F32)
    sig = jax.nn.sigmoid(gate_pre)
    active = gate_pre * sig
    hidden = (active * up_pre).astype(BF16)
    hidden_grad = nt(routed_grad, down_w)
    gate_grad = (hidden_grad * up_pre * sig * (1.0 + gate_pre * (1.0 - sig))).astype(BF16)
    up_grad = (hidden_grad * active).astype(BF16)
    terms = (nt(gate_grad, gate_w) + nt(up_grad, up_w)).astype(BF16)
    summed = lax.psum_scatter(terms, "tp", scatter_dimension=1, tiled=True)
    returned = lax.all_to_all(
        summed.reshape(senders, slots // senders, cols), "sp", 0, 0, tiled=True
    ).reshape(slots, cols)
    (mixer_cols,) = call(partial(combine_kernel, experts), [((rows, cols), BF16)], 100_000_000)(
        returned, cotangent, expert_ids
    )
    mixer_rows = lax.all_gather(mixer_cols, "tp", axis=1, tiled=True)
    norm_grad = jnp.dot(mixer_rows, w_out, preferred_element_type=F32)
    state_grad, xs_grad, x_grad, z_grad, run_grad, b_grad, c_grad = call(
        backward_kernel,
        [
            ((STATE, inner), BF16),
            ((rows, inner), F32),
            ((rows, inner), F32),
            ((rows, inner), BF16),
            ((rows, heads), F32),
            ((rows, STATE), F32),
            ((rows, STATE), F32),
        ],
        600_000_000,
    )(inner_x, inner_b, inner_c, gate_z, dt, run, run_t, skip, gain, mixed, state, norm_grad)
    state_grads = lax.all_gather(state_grad, "sp")
    depth = mixer_rows.shape[1] // senders
    mixer_blocks = jnp.swapaxes(mixer_rows.reshape(rows, senders, depth), 0, 1)
    mixer_all = lax.all_to_all(mixer_blocks, "sp", 0, 0, tiled=True).reshape(rows * senders, depth)
    grad_out = tn(mixer_all, norm_all)
    gate_weight_gradient = tn(routed_in, gate_grad).astype(BF16)[None]
    up_weight_gradient = tn(routed_in, up_grad).astype(BF16)[None]
    down_weight_gradient = tn(hidden, routed_grad).astype(BF16)[None]
    grad_inner_x, grad_inner_b, grad_step_raw = call(
        finish_kernel,
        [((rows, inner), BF16), ((rows, STATE), F32), ((rows, heads), F32)],
        300_000_000,
        [weight_rows],
    )(
        inner_x, inner_b, step_raw, dt, run, rate, state, state_grads, back, xs_grad, x_grad,
        run_grad, b_grad,
    )
    return (
        gate_weight_gradient, up_weight_gradient, down_weight_gradient, grad_out, grad_inner_x,
        grad_inner_b, c_grad, z_grad, grad_step_raw,
    )


def solution(mesh):
    row = P("sp", "tp")
    deep, flat, tall = P("sp", None, "tp"), P("sp", None), P("sp", "tp", None)
    return jax.shard_map(
        body,
        mesh=mesh,
        in_specs=(
            row, row, flat, flat, deep, deep, tall, row, row, row, row, row,
            P("tp"), P("tp"), P("tp"), P(None, "tp"),
        ),
        out_specs=(deep, deep, tall, row, row, row, row, row, row),
        check_vma=False,
    )
```

time: 392 us -> 268 us (0.68)
  waiting for transfers between devices: 168 us -> 112 us
  other arithmetic: 37.7 us -> 0.23 us
  matrix products: 53.3 us -> 19.3 us
  local copies, waits for them, and re-layouts: 38.6 us -> 15.8 us
  blocking collectives: 68.3 us -> 88.2 us
  Pallas kernels: 0 us -> 13.2 us
    reduce_scatter x2 -> x1, waiting for transfers between devices: 109 us -> 28.1 us  [body(): summed = lax.psum_scatter(terms, 'tp', scatter_dimension=1, tiled=True)]
    dot_general x24 -> x12, matrix products: 53.3 us -> 19.3 us  [the longest x4 10.5 us: tn(): lax.dot_general(a.astype(BF16), b.astype(BF16), (((0,), (0,)), ((), ())),...]
    all_to_all x2, blocking collectives: 39.4 us -> 61.2 us  [the longest x1 33 us: body(): lax.all_to_all(sent.reshape(senders, slots // senders, 2 * cols), 'sp', 0...]
    unnamed x1 -> x0, blocking collectives: 21.8 us -> none
    all_gather x0 -> x1, blocking collectives: none -> 20.5 us  [carries(): ends = lax.all_gather(last, axis)]
    all_gather x4, waiting for transfers between devices: 59.8 us -> 74.3 us  [the longest x1 31.7 us: body(): routed = lax.all_gather(routed, 'tp')]
    pallas_call x0 -> x6, Pallas kernels: none -> 13.2 us  [the longest x1 3.92 us: body(): call(finish_kernel, [((rows, inner), BF16), ((rows, STATE), F32), ((rows,...]
    convert_element_type x14 -> x0, other arithmetic: 10 us -> none  [the longest x8 5.25 us: step(): part[at].astype(own.dtype)]
  transfers between devices with their start and end apart: 7 -> 6, of which waited for: 5 -> 5; matrix products, arithmetic and copies ran while one was open for 26% -> 9% of each run, Pallas kernels for 0% -> 3%
where the time goes in v1:
time: 268 us; the launch traced here: 267 us
  waiting for transfers between devices  112 us (42%)
  blocking collectives  88.2 us (33%)
  matrix products  19.3 us (7%)
  local copies, waits for them, and re-layouts  15.8 us (6%)
  between operations  14.3 us (5%)
  Pallas kernels  13.2 us (5%)
  starting transfers between devices  4.53 us (2%)
    all_to_all x1, blocking collectives, body(): lax.all_to_all(sent.reshape(senders, slots // senders, 2 * cols), 'sp', 0...  33 us
    all_gather x1, waiting for transfers between devices, body(): routed = lax.all_gather(routed, 'tp')  31.7 us
    all_gather x1, waiting for transfers between devices, body(): state_grads = lax.all_gather(state_grad, 'sp')  30.3 us
    all_to_all x1, blocking collectives, body(): lax.all_to_all(summed.reshape(senders, slots // senders, cols), 'sp', 0,...  28.3 us
    reduce_scatter x1, waiting for transfers between devices, body(): summed = lax.psum_scatter(terms, 'tp', scatter_dimension=1, tiled=True)  28.1 us
    all_gather x1, blocking collectives, carries(): ends = lax.all_gather(last, axis)  20.5 us
    all_gather x1, waiting for transfers between devices, body(): fresh_all = lax.all_gather(fresh, 'sp')  12.4 us
    unnamed x93, local copies, waits for them, and re-layouts  11.4 us
  transfers between devices with their start and end apart: 6, of which 5 were waited for; matrix products, arithmetic and copies ran while one was open for 9% of the time, Pallas kernels for 3%

profile of v1, /device:TPU:0, one launch (start us, length us, event | category | flops | bytes accessed | tf_op | source)
XLA Modules:
  0.0 267.4 jit_solution(16126483471153247708)
XLA Ops:
  7.2 0.9 copy.84.ids_ref
  8.1 0.8 copy.85.weight_ref
  8.9 0.9 copy-done.4
  9.8 0.9 copy-done.7
  10.7 1.1 shard_map.223
  11.8 33.0 %all_to_all.15 = bf16[8,64,1024]{2,1,0:T(8,128)(2,1)} all-to-all(bf16[8,64,1024]{2,1,0:T(8,128)(2,1)S(1)} %bitcast.68), channel_id=1, replica_groups=mesh['sp'=8,'tp'=4] {'sp'}, dimensions={0} | all-to-all | bytes 2097152 | tf_op jit(solution)/shard_map/all_to_all | solution.py:290
  44.9 0.1 copy.96.b_ref
  45.0 0.1 copy.88.raw_ref
  45.2 0.2 reduce_window_sum.11.run_ref
  45.4 1.4 shard_map.225
  46.8 31.7 %all-gather.8.cloned.1.call-done = bf16[4,512,1024]{2,1,0:T(8,128)(2,1)} async-done(((bf16[1,512,1024]{2,1,0:T(8,128)(2,1)}), bf16[4,512,1024]{2,1,0:T(8,128)(2,1)}) %all-gather.8.cloned.1.call-update) | async-done | bytes 4194320 | tf_op jit(solution)/shard_map/all_gather | solution.py:293
  78.5 2.4 slice_bitcast_fusion.3
  81.0 0.9 fusion.7
  82.0 0.2 copy-done.29
  82.2 0.8 copy-done.14
  83.0 0.9 fusion.10
  84.0 0.4 copy-done.37
  84.4 0.8 multiply_convert_fusion.1
  85.3 0.7 fusion.5
  86.1 2.1 add_convert_fusion
  88.3 0.1 copy.97.c_ref
  88.5 20.5 %all-gather.2 = f32[8,1,16]{2,1,0:T(1,128)S(1)} all-gather(f32[1,1,16]{2,1,0:T(1,128)S(1)} %slice_bitcast_fusion.8), channel_id=1, replica_groups=mesh['sp'=8,'tp'=4] {'sp'}, dimensions={0}, use_global_device_ids=true | all-gather | bytes 576 | tf_op jit(solution)/shard_map/all_gather | solution.py:256
  109.0 0.1 fusion.3.coef_ref
  109.1 12.4 %all-gather.12.cloned.1.call-done = bf16[512,1024]{1,0:T(8,128)(2,1)} async-done(((bf16[64,1024]{1,0:T(8,128)(2,1)}), bf16[512,1024]{1,0:T(8,128)(2,1)}) %all-gather.12.cloned.1.call-update) | async-done | bytes 1048592 | tf_op jit(solution)/shard_map/all_gather | solution.py:284
  121.5 1.2 copy-done.2
  122.7 3.1 %shard_map.226 = (bf16[128,1024]{1,0:T(8,128)(2,1)}, f32[128,1024]{1,0:T(8,128)S(1)}, f32[64,1024]{1,0:T(8,128)S(1)}) custom-call(bf16[128,1024]{1,0:T(8,128)(2,1)S(1)} %copy-done.1, bf16[128,64]{1,0:T(8,128)(2,1)S(1)} %copy.96.b_ref, bf16[128,64]{1,0:T(8,128)(2,1)S(1)} %copy.97.c_ref, bf16[128,1024]{1,0:T(8,128)(2,1)S(1)} %copy-done.6, ...), custom_call_target="tpu_custom_call" | custom-call | flops 300000000 | bytes 4000000 | tf_op jit(solution)/shard_map/pallas_call | solution.py:296
  125.9 28.1 %reduce-scatter.2.cloned.1.call-done = bf16[512,512]{1,0:T(8,128)(2,1)} async-done(((bf16[512,2048]{1,0:T(8,128)(2,1)}), bf16[512,512]{1,0:T(8,128)(2,1)}) %reduce-scatter.2.cloned.1.call-update) | async-done | bytes 524304 | tf_op jit(solution)/shard_map/reduce_scatter | solution.py:316
  153.9 28.3 %all_to_all.16 = bf16[8,64,512]{2,1,0:T(8,128)(2,1)S(1)} all-to-all(bf16[8,64,512]{2,1,0:T(8,128)(2,1)} %bitcast.82), channel_id=1, replica_groups=mesh['sp'=8,'tp'=4] {'sp'}, dimensions={0} | all-to-all | bytes 1048576 | tf_op jit(solution)/shard_map/all_to_all | solution.py:317
  182.2 0.6 shard_map.224
  182.8 6.5 %all_gather.25 = bf16[128,2048]{1,0:T(8,128)(2,1)S(1)} all-gather(bf16[128,512]{1,0:T(8,128)(2,1)S(1)} %shard_map.224), channel_id=1, replica_groups=mesh['sp'=8,'tp'=4] {'tp'}, dimensions={1}, use_global_device_ids=true | all-gather | bytes 655360 | tf_op jit(solution)/shard_map/all_gather | solution.py:323
  189.3 3.1 %fusion.26.up_ref = f32[128,1024]{1,0:T(8,128)S(1)} fusion(bf16[128,2048]{1,0:T(8,128)(2,1)S(1)} %all_gather.25, bf16[2048,1024]{1,0:T(8,128)(2,1)} %param.31), kind=kOutput, calls=%fused_computation.51 | convolution fusion | flops 536870912 | bytes 5242880 | tf_op jit(solution)/shard_map/dot_general | solution.py:324
  192.5 1.0 copy-done.12
  193.5 3.1 %shard_map.227 = (bf16[64,1024]{1,0:T(8,128)(2,1)}, f32[128,1024]{1,0:T(8,128)S(1)}, f32[128,1024]{1,0:T(8,128)S(1)}, bf16[128,1024]{1,0:T(8,128)(2,1)}, f32[128...) custom-call(bf16[128,1024]{1,0:T(8,128)(2,1)S(1)} %copy-done.1, bf16[128,64]{1,0:T(8,128)(2,1)S(1)} %copy.96.b_ref, ...), custom_call_target="tpu_custom_call" | custom-call | flops 600000000 | bytes 4000000 | tf_op jit(solution)/shard_map/pallas_call | solution.py:325
  196.7 0.1 fusion.4.coef_ref
  196.8 1.9 copy.108
  198.8 4.3 %all-to-all-start.2 = ((bf16[8,128,256]{2,1,0:T(8,128)(2,1)}), bf16[8,128,256]{2,1,0:T(8,128)(2,1)}, u32[]{:S(2)}, u32[]{:S(2)}) async-start(bf16[8,128,256]{2,1,0:T(8,128)(2,1)} %bitcast.81), calls=%async_computation.3 | async-start | bytes 1048576 | tf_op jit(solution)/shard_map/all_to_all | solution.py:341
  203.2 3.5 %fusion = bf16[1,2048,256]{2,1,0:T(8,128)(2,1)} fusion(bf16[512,256]{1,0:T(8,128)(2,1)} %copy-done.31, bf16[512,512]{1,0:T(8,128)(2,1)} %copy-done.23, bf16[512,512]{1,0:T(8,128)(2,1)} %copy-done.25, bf16[512,512]{1,0:T(8,128)(2,1)} %copy-done.27, bf16[512,512]{1,0:T(8,128)(2,1)} %copy-done.29), kind=kOutput, calls=%fused_computation.4 | convolution fusion | flops 545783808 | bytes 3407872 | tf_op jit(solution)/shard_map/dot_general | solution.py:34
  206.7 1.7 fusion.1
  208.5 0.3 copy-done.41
  208.7 1.7 fusion.2
  210.5 0.7 copy.103
  211.2 9.3 %all-to-all-done.2 = bf16[8,128,256]{2,1,0:T(8,128)(2,1)} async-done(((bf16[8,128,256]{2,1,0:T(8,128)(2,1)}), bf16[8,128,256]{2,1,0:T(8,128)(2,1)}, u32[]{:S(2)}, u32[]{:S(2)}) %all-to-all-start.2) | async-done | bytes 524320 | tf_op jit(solution)/shard_map/all_to_all | solution.py:341
  220.4 3.5 %fusion.25 = f32[256,1024]{1,0:T(8,128)} fusion(bf16[1024,256]{1,0:T(8,128)(2,1)} %bitcast.19, bf16[1024,1024]{1,0:T(8,128)(2,1)} %all-gather.10.cloned.1.call-done), kind=kOutput, calls=%fused_computation.50 | convolution fusion | flops 536870912 | bytes 3670016 | tf_op jit(solution)/shard_map/dot_general | solution.py:34
  224.0 30.3 %all-gather.14.cloned.1.call-done = bf16[512,1024]{1,0:T(8,128)(2,1)} async-done(((bf16[64,1024]{1,0:T(8,128)(2,1)}), bf16[512,1024]{1,0:T(8,128)(2,1)}) %all-gather.14.cloned.1.call-update) | async-done | bytes 1048592 | tf_op jit(solution)/shard_map/all_gather | solution.py:338
  254.3 1.2 copy-done.3
  255.5 3.9 %shard_map.228 = (bf16[128,1024]{1,0:T(8,128)(2,1)}, f32[128,64]{1,0:T(8,128)S(1)}, f32[128,16]{1,0:T(8,128)S(1)}) custom-call(bf16[128,1024]{1,0:T(8,128)(2,1)S(1)} %copy-done.1, bf16[128,64]{1,0:T(8,128)(2,1)S(1)} %copy.96.b_ref, f32[128,16]{1,0:T(8,128)S(1)} %copy.88.raw_ref, f32[128,16]{1,0:T(8,128)S(1)} %get-tuple-element.82.dt_ref, ...), custom_call_target="tpu_custom_call" | custom-call | flops 300000000 | bytes 4000000 | tf_op jit(solution)/shard_map/pallas_call | solution.py:346
  259.5 0.7 copy.102
  260.2 0.7 copy.104
  (91 shorter events, 0.7 us)
Async XLA Ops:
  7.2 73.8 %copy-start = (bf16[1,2048,256]{2,1,0:T(8,128)(2,1)S(1)}, bf16[1,2048,256]{2,1,0:T(8,128)(2,1)}, u32[]{:S(2)}) copy-start(bf16[1,2048,256]{2,1,0:T(8,128)(2,1)} %param.20) | copy-start | bytes 3145732
  7.2 38.2 %copy-start.1 = (bf16[128,1024]{1,0:T(8,128)(2,1)S(1)}, bf16[128,1024]{1,0:T(8,128)(2,1)}, u32[]{:S(2)}) copy-start(bf16[128,1024]{1,0:T(8,128)(2,1)} %x_ref.9) | copy-start | bytes 786436
  7.2 71.3 %all-gather.8.cloned.1.call-start = ((), (), s32[]{:S(2)}) async-start(), calls=%async_computation.4 | async-start | bytes 5242880 | tf_op jit(solution)/shard_map/all_gather | solution.py:293
  8.9 0.9 copy-start.4
  9.8 0.9 copy-start.7
  10.7 34.2 %copy-start.34 = (bf16[128,64]{0,1:T(8,128)(2,1)S(1)}, bf16[128,64]{0,1:T(8,128)(2,1)}, u32[]{:S(2)}) copy-start(bf16[128,64]{0,1:T(8,128)(2,1)} %param.24) | copy-start | bytes 49156
  10.7 34.3 %copy-start.36 = (f32[128,16]{0,1:T(8,128)S(1)}, f32[128,16]{0,1:T(8,128)}, u32[]{:S(2)}) copy-start(f32[128,16]{0,1:T(8,128)} %param.27) | copy-start | bytes 24580
  10.7 34.4 %copy-start.9 = (f32[16]{0:T(128)S(1)}, f32[16]{0:T(128)}, u32[]{:S(2)}) copy-start(f32[16]{0:T(128)} %param.28) | copy-start | bytes 196
  44.8 76.6 %all-gather.12.cloned.1.call-start = ((), (), s32[]{:S(2)}) async-start(), calls=%async_computation.7 | async-start | bytes 1179648 | tf_op jit(solution)/shard_map/all_gather | solution.py:284
  46.8 107.2 %reduce-scatter.2.cloned.1.call-start = ((), (), s32[]{:S(2)}) async-start(), calls=%async_computation.5 | async-start | bytes 2621440 | tf_op jit(solution)/shard_map/reduce_scatter | solution.py:316
  80.9 1.0 copy-start.23
  80.9 1.0 copy-start.25
  80.9 1.1 copy-start.27
  80.9 1.3 copy-start.29
  80.9 3.0 %copy-start.15 = (bf16[512,512]{1,0:T(8,128)(2,1)}, bf16[512,512]{1,0:T(8,128)(2,1)S(1)}, u32[]{:S(2)}) copy-start(bf16[512,512]{1,0:T(8,128)(2,1)S(1)} %get-tuple-element.71) | copy-start | bytes 1572868
  80.9 3.0 %copy-start.17 = (bf16[512,512]{1,0:T(8,128)(2,1)}, bf16[512,512]{1,0:T(8,128)(2,1)S(1)}, u32[]{:S(2)}) copy-start(bf16[512,512]{1,0:T(8,128)(2,1)S(1)} %get-tuple-element.72) | copy-start | bytes 1572868
  81.0 3.0 %copy-start.19 = (bf16[512,512]{1,0:T(8,128)(2,1)}, bf16[512,512]{1,0:T(8,128)(2,1)S(1)}, u32[]{:S(2)}) copy-start(bf16[512,512]{1,0:T(8,128)(2,1)S(1)} %get-tuple-element.73) | copy-start | bytes 1572868
  81.0 3.0 %copy-start.21 = (bf16[512,512]{1,0:T(8,128)(2,1)}, bf16[512,512]{1,0:T(8,128)(2,1)S(1)}, u32[]{:S(2)}) copy-start(bf16[512,512]{1,0:T(8,128)(2,1)S(1)} %get-tuple-element.74) | copy-start | bytes 1572868
  81.0 2.0 copy-start.14
  83.0 1.0 copy-start.38
  83.0 1.4 copy-start.37
  83.9 1.3 copy-start.40
  85.3 0.8 copy-start.31
  85.3 0.8 copy-start.32
  86.1 2.2 copy-start.35
  86.1 35.4 %copy-start.6 = (bf16[128,1024]{1,0:T(8,128)(2,1)S(1)}, bf16[128,1024]{1,0:T(8,128)(2,1)}, u32[]{:S(2)}) copy-start(bf16[128,1024]{1,0:T(8,128)(2,1)} %z_ref.3) | copy-start | bytes 786436
  86.1 35.4 %copy-start.8 = (f32[1024]{0:T(1024)S(1)}, f32[1024]{0:T(1024)}, u32[]{:S(2)}) copy-start(f32[1024]{0:T(1024)} %param.30) | copy-start | bytes 12292
  86.1 35.4 %copy-start.10 = (f32[16]{0:T(128)S(1)}, f32[16]{0:T(128)}, u32[]{:S(2)}) copy-start(f32[16]{0:T(128)} %param.29) | copy-start | bytes 196
  88.2 94.0 %copy-start.5 = (bf16[128,512]{1,0:T(8,128)(2,1)S(1)}, bf16[128,512]{1,0:T(8,128)(2,1)}, u32[]{:S(2)}) copy-start(bf16[128,512]{1,0:T(8,128)(2,1)} %cot_ref.3) | copy-start | bytes 393220
  88.2 122.9 %all-gather.10.cloned.1.call-start = ((), (), s32[]{:S(2)}) async-start(), calls=%async_computation.6 | async-start | bytes 2359296 | tf_op jit(solution)/shard_map/all_gather | solution.py:302
  121.5 1.2 copy-start.2
  125.8 66.7 %copy-start.11 = (f32[128,1024]{1,0:T(8,128)}, f32[128,1024]{1,0:T(8,128)S(1)}, u32[]{:S(2)}) copy-start(f32[128,1024]{1,0:T(8,128)S(1)} %get-tuple-element.24.mixed_ref) | copy-start | bytes 1572868
  125.8 128.5 %all-gather.14.cloned.1.call-start = ((), (), s32[]{:S(2)}) async-start(), calls=%async_computation.8 | async-start | bytes 1179648 | tf_op jit(solution)/shard_map/all_gather | solution.py:338
  189.3 3.1 %copy-start.13 = (bf16[128,2048]{1,0:T(8,128)(2,1)}, bf16[128,2048]{1,0:T(8,128)(2,1)S(1)}, u32[]{:S(2)}) copy-start(bf16[128,2048]{1,0:T(8,128)(2,1)S(1)} %all_gather.25) | copy-start | bytes 1572868
  192.5 1.0 copy-start.12
  198.8 21.7 %all-to-all-start.2 = ((bf16[8,128,256]{2,1,0:T(8,128)(2,1)}), bf16[8,128,256]{2,1,0:T(8,128)(2,1)}, u32[]{:S(2)}, u32[]{:S(2)}) async-start(bf16[8,128,256]{2,1,0:T(8,128)(2,1)} %bitcast.81), calls=%async_computation.3 | async-start | bytes 1048576 | tf_op jit(solution)/shard_map/all_to_all | solution.py:341
  203.1 3.5 %copy-start.24 = (bf16[512,512]{1,0:T(8,128)(2,1)S(1)}, bf16[512,512]{1,0:T(8,128)(2,1)}, u32[]{:S(2)}) copy-start(bf16[512,512]{1,0:T(8,128)(2,1)} %copy-done.23) | copy-start | bytes 1572868
  203.1 3.5 %copy-start.26 = (bf16[512,512]{1,0:T(8,128)(2,1)S(1)}, bf16[512,512]{1,0:T(8,128)(2,1)}, u32[]{:S(2)}) copy-start(bf16[512,512]{1,0:T(8,128)(2,1)} %copy-done.25) | copy-start | bytes 1572868
  203.1 3.5 %copy-start.28 = (bf16[512,512]{1,0:T(8,128)(2,1)S(1)}, bf16[512,512]{1,0:T(8,128)(2,1)}, u32[]{:S(2)}) copy-start(bf16[512,512]{1,0:T(8,128)(2,1)} %copy-done.27) | copy-start | bytes 1572868
  203.1 3.5 %copy-start.30 = (bf16[512,512]{1,0:T(8,128)(2,1)S(1)}, bf16[512,512]{1,0:T(8,128)(2,1)}, u32[]{:S(2)}) copy-start(bf16[512,512]{1,0:T(8,128)(2,1)} %copy-done.29) | copy-start | bytes 1572868
  203.1 3.5 %copy-start.33 = (bf16[512,256]{1,0:T(8,128)(2,1)S(1)}, bf16[512,256]{1,0:T(8,128)(2,1)}, u32[]{:S(2)}) copy-start(bf16[512,256]{1,0:T(8,128)(2,1)} %copy-done.32) | copy-start | bytes 786436
  206.6 1.8 copy-start.16
  206.7 1.8 copy-start.18
  206.7 1.8 copy-start.20
  206.7 1.8 copy-start.22
  206.7 1.8 copy-start.39
  206.7 2.1 copy-start.41
  254.3 1.2 copy-start.3
Sparse Core Ops, SparseCore 0:
  45.0 33.4 all-gather.7
  81.2 40.2 all-gather.11
  124.0 29.8 reduce-scatter.1
  155.9 54.7 all-gather.9
  212.7 41.5 all-gather.13

commit v2 on v1

--- a/solution.py
+++ b/solution.py
@@ -234,21 +234,247 @@
 
 
 def dispatch_kernel(experts, x_ref, cot_ref, ids_ref, weight_ref, out_ref):
-    slots = out_ref.shape[0]
+    slots = out_ref.shape[1]
     cols = x_ref.shape[1]
     found = picks(ids_ref[...], slots, experts)
     cot = cot_ref[...].astype(F32)
     total = jnp.zeros((slots, cols), F32)
     for k, one in enumerate(found):
         total += tn(one, (cot * weight_ref[:, k : k + 1]).astype(BF16))
-    out_ref[:, :cols] = tn(sum(found), x_ref[...]).astype(BF16)
-    out_ref[:, cols:] = total.astype(BF16)
+    out_ref[0] = tn(sum(found), x_ref[...]).astype(BF16)
+    out_ref[1] = total.astype(BF16)
 
 
 def combine_kernel(experts, back_ref, cot_ref, ids_ref, out_ref):
     found = picks(ids_ref[...], back_ref.shape[0], experts)
     moe_grad = nn(sum(found), back_ref[...])
     out_ref[...] = (cot_ref[...].astype(F32) + moe_grad).astype(BF16)
+
+
+MESH = pl.DeviceIdType.MESH
+
+
+def greet(count, me, others):
+    barrier = pltpu.get_barrier_semaphore()
+
+    def one(d, _):
+        pl.semaphore_signal(
+            barrier, inc=1, device_id={"sp": lax.rem(me + d, count)}, device_id_type=MESH
+        )
+        return 0
+
+    lax.fori_loop(1, count, one, 0)
+    for other in others:
+        pl.semaphore_signal(barrier, inc=1, device_id={"tp": other}, device_id_type=MESH)
+    pl.semaphore_wait(barrier, count - 1 + len(others))
+
+
+def partners():
+    t = lax.axis_index("tp")
+    half = lax.axis_size("tp") // 2
+    far = lax.rem(t + half, 2 * half)
+    near = t + 1 - 2 * lax.rem(t, 2)
+    return t, far, near
+
+
+def route_kernel(
+    count, sent_ref, out_ref, own_sem, sp_send, sp_recv, far_send, far_recv, near_send, near_recv
+):
+    cols = sent_ref.shape[3]
+    me = lax.axis_index("sp")
+    t, far, near = partners()
+
+    def at(block, place):
+        return out_ref.at[:, block, :, pl.ds(pl.multiple_of(place * cols, 128), cols)]
+
+    def over_sp(d):
+        to = lax.rem(me + d, count)
+        return pltpu.make_async_remote_copy(
+            src_ref=sent_ref.at[:, to], dst_ref=at(me, t), send_sem=sp_send.at[d],
+            recv_sem=sp_recv.at[d], device_id={"sp": to}, device_id_type=MESH,
+        )
+
+    def over_far(d):
+        block = lax.rem(me - d + count, count)
+        return pltpu.make_async_remote_copy(
+            src_ref=at(block, t), dst_ref=at(block, t), send_sem=far_send.at[d],
+            recv_sem=far_recv.at[d], device_id={"tp": far}, device_id_type=MESH,
+        )
+
+    def over_near(d, k):
+        block = lax.rem(me - d + count, count)
+        place = far if k else t
+        return pltpu.make_async_remote_copy(
+            src_ref=at(block, place), dst_ref=at(block, place), send_sem=near_send.at[k, d],
+            recv_sem=near_recv.at[k, d], device_id={"tp": near}, device_id_type=MESH,
+        )
+
+    own = pltpu.make_async_copy(sent_ref.at[:, me], at(me, t), own_sem)
+    own.start()
+    greet(count, me, (far, near))
+
+    def each(body, start=0):
+        def step(d, _):
+            body(d)
+            return 0
+
+        lax.fori_loop(start, count, step, 0)
+
+    each(lambda d: over_sp(d).start(), 1)
+    own.wait()
+    over_far(0).start()
+    over_near(0, 0).start()
+
+    def arrived(d):
+        over_sp(d).wait_recv()
+        over_far(d).start()
+        over_near(d, 0).start()
+
+    each(arrived, 1)
+
+    def crossed(d):
+        over_far(d).wait_recv()
+        over_near(d, 1).start()
+
+    each(crossed)
+
+    def close(d):
+        over_far(d).wait_send()
+        over_near(d, 0).wait()
+        over_near(d, 1).wait()
+
+    each(close)
+    each(lambda d: over_sp(d).wait_send(), 1)
+
+
+def route(sent, tp):
+    two, count, capacity, cols = sent.shape
+    dma = pltpu.SemaphoreType.DMA
+    return pl.pallas_call(
+        partial(route_kernel, count),
+        out_shape=jax.ShapeDtypeStruct((two, count, capacity, tp * cols), BF16),
+        in_specs=[pl.BlockSpec(memory_space=pltpu.VMEM)],
+        out_specs=pl.BlockSpec(memory_space=pltpu.VMEM),
+        scratch_shapes=[
+            dma(()), dma((count,)), dma((count,)), dma((count,)), dma((count,)),
+            dma((2, count)), dma((2, count)),
+        ],
+        cost_estimate=pl.CostEstimate(
+            flops=10_000_000_000, bytes_accessed=8_000_000, transcendentals=0
+        ),
+        compiler_params=pltpu.CompilerParams(
+            collective_id=0, has_side_effects=True, vmem_limit_bytes=32 * 1024 * 1024
+        ),
+    )(sent)
+
+
+def fold_kernel(
+    count, terms_ref, out_ref, close_ref, pair_ref, away_ref, full_ref,
+    own_sem, near_send, near_recv, far_send, far_recv, sp_send, sp_recv,
+):
+    cols = out_ref.shape[2]
+    me = lax.axis_index("sp")
+    t, far, near = partners()
+    far_near = near + far - t
+
+    def mine(ref, block, place):
+        return ref.at[block, :, pl.ds(pl.multiple_of(place * cols, 128), cols)]
+
+    def block_at(d):
+        return lax.rem(me + d, count)
+
+    def over_near(d, k):
+        return pltpu.make_async_remote_copy(
+            src_ref=mine(terms_ref, block_at(d), far_near if k else near),
+            dst_ref=close_ref.at[k, d], send_sem=near_send.at[k, d],
+            recv_sem=near_recv.at[k, d], device_id={"tp": near}, device_id_type=MESH,
+        )
+
+    def over_far(d):
+        return pltpu.make_async_remote_copy(
+            src_ref=pair_ref.at[d], dst_ref=away_ref.at[d], send_sem=far_send.at[d],
+            recv_sem=far_recv.at[d], device_id={"tp": far}, device_id_type=MESH,
+        )
+
+    def over_sp(d):
+        return pltpu.make_async_remote_copy(
+            src_ref=full_ref.at[d], dst_ref=out_ref.at[me], send_sem=sp_send.at[d],
+            recv_sem=sp_recv.at[d], device_id={"sp": block_at(d)}, device_id_type=MESH,
+        )
+
+    def each(body, start=0):
+        def step(d, _):
+            body(d)
+            return 0
+
+        lax.fori_loop(start, count, step, 0)
+
+    greet(count, me, (far, near))
+    order = lambda d: lax.rem(d + 1, count)
+
+    def begin(d):
+        over_near(order(d), 1).start()
+        over_near(order(d), 0).start()
+
+    each(begin)
+
+    def pair(i):
+        d = order(i)
+        over_near(d, 1).wait_recv()
+        here = mine(terms_ref, block_at(d), far)[...].astype(F32)
+        pair_ref[d] = (here + close_ref[1, d].astype(F32)).astype(BF16)
+        over_far(d).start()
+
+    each(pair)
+
+    def total(d):
+        over_near(d, 0).wait_recv()
+        over_far(d).wait_recv()
+        here = mine(terms_ref, block_at(d), t)[...].astype(F32)
+        here = here + close_ref[0, d].astype(F32) + away_ref[d].astype(F32)
+        full_ref[d] = here.astype(BF16)
+
+    def send(d):
+        total(d)
+        over_sp(d).start()
+
+    each(send, 1)
+    total(0)
+    own = pltpu.make_async_copy(full_ref.at[0], out_ref.at[me], own_sem)
+    own.start()
+
+    def close(d):
+        over_near(d, 0).wait_send()
+        over_near(d, 1).wait_send()
+        over_far(d).wait_send()
+
+    each(close)
+    own.wait()
+    each(lambda d: over_sp(d).wait(), 1)
+
+
+def fold(terms, tp):
+    count, capacity, width = terms.shape
+    cols = width // tp
+    dma = pltpu.SemaphoreType.DMA
+    part = (count, capacity, cols)
+    return pl.pallas_call(
+        partial(fold_kernel, count),
+        out_shape=jax.ShapeDtypeStruct(part, BF16),
+        in_specs=[pl.BlockSpec(memory_space=pltpu.VMEM)],
+        out_specs=pl.BlockSpec(memory_space=pltpu.VMEM),
+        scratch_shapes=[
+            pltpu.VMEM((2,) + part, BF16), pltpu.VMEM(part, BF16), pltpu.VMEM(part, BF16),
+            pltpu.VMEM(part, BF16), dma(()), dma((2, count)), dma((2, count)), dma((count,)),
+            dma((count,)), dma((count,)), dma((count,)),
+        ],
+        cost_estimate=pl.CostEstimate(
+            flops=10_000_000_000, bytes_accessed=4_000_000, transcendentals=0
+        ),
+        compiler_params=pltpu.CompilerParams(
+            collective_id=1, has_side_effects=True, vmem_limit_bytes=32 * 1024 * 1024
+        ),
+    )(terms)
 
 
 def carries(last, axis):
@@ -284,13 +510,13 @@
     fresh_all = lax.all_gather(fresh, "sp")
     fore, back = carries(run[-1], "sp")
 
-    (sent,) = call(partial(dispatch_kernel, experts), [((slots, 2 * cols), BF16)], 200_000_000)(
+    (sent,) = call(partial(dispatch_kernel, experts), [((2, slots, cols), BF16)], 200_000_000)(
         moe_input, cotangent, expert_ids, routing_weights
     )
-    routed = lax.all_to_all(
-        sent.reshape(senders, slots // senders, 2 * cols), "sp", 0, 0, tiled=True
-    ).reshape(slots, 2 * cols)
-    routed = lax.all_gather(routed, "tp")
+    tp = lax.axis_size("tp")
+    routed = route(sent.reshape(2, senders, slots // senders, cols), tp)
+    routed = routed.reshape(2, slots, tp * cols)
+    routed_in, routed_grad = routed[0], routed[1]
 
     weight_rows = pltpu.VMEM((senders, inner), F32)
     norm_rows, mixed, state = call(
@@ -301,8 +527,6 @@
     )(inner_x, inner_b, inner_c, gate_z, dt, run, run_t, skip, gain, fresh_all, fore)
     norm_all = lax.all_gather(norm_rows, "sp", axis=0, tiled=True)
 
-    routed_in = jnp.concatenate([routed[k, :, :cols] for k in range(routed.shape[0])], axis=1)
-    routed_grad = jnp.concatenate([routed[k, :, cols:] for k in range(routed.shape[0])], axis=1)
     gate_w, up_w, down_w = gate_weight[0], up_weight[0], down_weight[0]
     gate_pre = jnp.dot(routed_in, gate_w, preferred_element_type=F32)
     up_pre = jnp.dot(routed_in, up_w, preferred_element_type=F32)
@@ -313,10 +537,7 @@
     gate_grad = (hidden_grad * up_pre * sig * (1.0 + gate_pre * (1.0 - sig))).astype(BF16)
     up_grad = (hidden_grad * active).astype(BF16)
     terms = (nt(gate_grad, gate_w) + nt(up_grad, up_w)).astype(BF16)
-    summed = lax.psum_scatter(terms, "tp", scatter_dimension=1, tiled=True)
-    returned = lax.all_to_all(
-        summed.reshape(senders, slots // senders, cols), "sp", 0, 0, tiled=True
-    ).reshape(slots, cols)
+    returned = fold(terms.reshape(senders, slots // senders, tp * cols), tp).reshape(slots, cols)
     (mixer_cols,) = call(partial(combine_kernel, experts), [((rows, cols), BF16)], 100_000_000)(
         returned, cotangent, expert_ids
     )

time: 268 us -> 237 us (0.88)
  Pallas kernels: 13.2 us -> 73.2 us
  blocking collectives: 88.2 us -> 31.1 us
  waiting for transfers between devices: 112 us -> 72.5 us
  local copies, waits for them, and re-layouts: 15.8 us -> 18.7 us
    all_to_all x2 -> x0, blocking collectives: 61.2 us -> none  [the longest x1 33 us: body(): lax.all_to_all(sent.reshape(senders, slots // senders, 2 * cols), 'sp', 0...]
    pallas_call x1 -> x3, Pallas kernels: 1.1 us -> 61.9 us  [the longest x1 42.7 us: route(): pl.pallas_call(partial(route_kernel, count), out_shape=jax.ShapeDtypeStru...]
    all_gather x1, waiting for transfers between devices: 0.01 us -> 43.5 us  [body(): norm_all = lax.all_gather(norm_rows, 'sp', axis=0, tiled=True)]
    all_gather x1 -> x0, waiting for transfers between devices: 31.7 us -> none  [body(): routed = lax.all_gather(routed, 'tp')]
    reduce_scatter x1 -> x0, waiting for transfers between devices: 28.1 us -> none  [body(): summed = lax.psum_scatter(terms, 'tp', scatter_dimension=1, tiled=True)]
    all_gather x1, waiting for transfers between devices: 12.4 us -> 0.02 us  [body(): fresh_all = lax.all_gather(fresh, 'sp')]
    all_to_all x1, waiting for transfers between devices: 9.26 us -> 0.01 us  [body(): lax.all_to_all(mixer_blocks, 'sp', 0, 0, tiled=True)]
    unnamed x93 -> x77, local copies, waits for them, and re-layouts: 11.4 us -> 16.2 us
  transfers between devices with their start and end apart: 6 -> 4, of which waited for: 5 -> 2; matrix products, arithmetic and copies ran while one was open for 9% -> 9% of each run, Pallas kernels for 3% -> 28%
where the time goes in v2:
time: 237 us; the launch traced here: 236 us
  Pallas kernels  73.2 us (31%)
  waiting for transfers between devices  72.5 us (31%)
  blocking collectives  31.1 us (13%)
  matrix products  19.5 us (8%)
  local copies, waits for them, and re-layouts  18.7 us (8%)
  between operations  14.1 us (6%)
  starting transfers between devices  6.57 us (3%)
    all_gather x1, waiting for transfers between devices, body(): norm_all = lax.all_gather(norm_rows, 'sp', axis=0, tiled=True)  43.5 us
    pallas_call x1, Pallas kernels, route(): pl.pallas_call(partial(route_kernel, count), out_shape=jax.ShapeDtypeStru...  42.7 us
    all_gather x1, waiting for transfers between devices, body(): state_grads = lax.all_gather(state_grad, 'sp')  28.4 us
    all_gather x1, blocking collectives, carries(): ends = lax.all_gather(last, axis)  23.9 us
    pallas_call x1, Pallas kernels, fold(): pl.pallas_call(partial(fold_kernel, count), out_shape=jax.ShapeDtypeStruc...  18.1 us
    unnamed x77, local copies, waits for them, and re-layouts  16.2 us
    dot_general x4, matrix products, tn(): lax.dot_general(a.astype(BF16), b.astype(BF16), (((0,), (0,)), ((), ())),...  10.5 us
    all_gather x1, blocking collectives, body(): mixer_rows = lax.all_gather(mixer_cols, 'tp', axis=1, tiled=True)  7.16 us
  transfers between devices with their start and end apart: 4, of which 2 were waited for; matrix products, arithmetic and copies ran while one was open for 9% of the time, Pallas kernels for 28%

profile of v2, /device:TPU:0, one launch (start us, length us, event | category | flops | bytes accessed | tf_op | source)
XLA Modules:
  0.0 236.4 jit_solution(10011407025306254557)
XLA Ops:
  7.2 0.9 copy.96.b_ref
  8.1 0.8 copy.88.raw_ref
  8.9 0.7 negate_multiply_fusion
  9.8 0.9 copy-done.1
  10.8 1.4 shard_map.227
  12.3 0.8 copy.84.ids_ref
  13.1 0.8 copy.85.weight_ref
  13.9 0.9 copy-done.5
  14.8 0.9 copy-done.9
  15.7 1.1 shard_map.223
  16.8 42.7 %shard_map.224 = bf16[2,8,64,2048]{3,2,1,0:T(8,128)(2,1)S(1)} custom-call(bf16[2,8,64,512]{3,2,1,0:T(8,128)(2,1)S(1)} %bitcast.62), custom_call_target="tpu_custom_call" | custom-call | flops 10000000000 | bytes 8000000 | tf_op jit(solution)/shard_map/pallas_call | solution.py:353
  59.5 0.6 fusion.23
  60.1 0.7 fusion.7
  60.8 1.3 copy-done.21
  62.1 0.7 fusion.10
  62.8 0.6 copy-done.33
  63.5 0.8 multiply_convert_fusion.1
  64.4 0.7 copy-done.26
  65.0 2.7 %fusion.5 = f32[512,2048]{1,0:T(8,128)} fusion(bf16[512,256]{1,0:T(8,128)(2,1)S(1)} %get-tuple-element.74, bf16[1,2048,256]{2,1,0:T(8,128)(2,1)S(1)} %copy-done), kind=kOutput, calls=%fused_computation.11 | convolution fusion | flops 536870912 | bytes 5505024 | tf_op jit(solution)/shard_map/dot_general | solution.py:40
  67.9 23.9 %all-gather.2 = f32[8,1,16]{2,1,0:T(1,128)S(1)} all-gather(f32[1,1,16]{2,1,0:T(1,128)S(1)} %slice_bitcast_fusion), channel_id=1, replica_groups=mesh['sp'=8,'tp'=4] {'sp'}, dimensions={0}, use_global_device_ids=true | all-gather | bytes 576 | tf_op jit(solution)/shard_map/all_gather | solution.py:482
  91.8 3.0 %add_convert_fusion = bf16[512,2048]{1,0:T(8,128)(2,1)S(1)} fusion(f32[512,2048]{1,0:T(8,128)} %fusion.5, bf16[512,256]{1,0:T(8,128)(2,1)S(1)} %get-tuple-element.73, bf16[1,2048,256]{2,1,0:T(8,128)(2,1)S(1)} %copy-done.21), kind=kOutput, calls=%fused_computation | convolution fusion | flops 538968064 | bytes 7602176 | tf_op jit(solution)/shard_map/dot_general | solution.py:40
  94.8 18.1 %shard_map.225 = bf16[8,64,512]{2,1,0:T(8,128)(2,1)S(1)} custom-call(bf16[8,64,2048]{2,1,0:T(8,128)(2,1)S(1)} %bitcast.59), custom_call_target="tpu_custom_call" | custom-call | flops 10000000000 | bytes 4000000 | tf_op jit(solution)/shard_map/pallas_call | solution.py:461
  112.9 0.6 shard_map.226
  113.6 7.2 %all_gather.21 = bf16[128,2048]{1,0:T(8,128)(2,1)S(1)} all-gather(bf16[128,512]{1,0:T(8,128)(2,1)S(1)} %shard_map.226), channel_id=1, replica_groups=mesh['sp'=8,'tp'=4] {'tp'}, dimensions={1}, use_global_device_ids=true | all-gather | bytes 655360 | tf_op jit(solution)/shard_map/all_gather | solution.py:544
  120.9 0.7 fusion.25.up_ref
  121.7 0.2 copy-done.2
  121.9 1.2 copy-done.3
  123.1 0.9 copy-done.8
  124.1 2.3 shard_map.228
  126.4 0.7 copy-done.7
  127.1 3.1 %shard_map.229 = (bf16[64,1024]{1,0:T(8,128)(2,1)}, f32[128,1024]{1,0:T(8,128)S(1)}, f32[128,1024]{1,0:T(8,128)S(1)}, bf16[128,1024]{1,0:T(8,128)(2,1)}, f32[128...) custom-call(bf16[128,1024]{1,0:T(8,128)(2,1)S(1)} %copy-done.2, bf16[128,64]{1,0:T(8,128)(2,1)S(1)} %copy.96.b_ref, ...), custom_call_target="tpu_custom_call" | custom-call | flops 600000000 | bytes 4000000 | tf_op jit(solution)/shard_map/pallas_call | solution.py:546
  130.2 0.6 copy-done.10
  130.9 0.2 all-gather.7.cloned.1.call-start
  131.1 0.5 all-gather.7.cloned.1.call-update
  131.6 1.9 copy.108
  133.5 6.3 %all-to-all-start = ((bf16[8,128,256]{2,1,0:T(8,128)(2,1)}), bf16[8,128,256]{2,1,0:T(8,128)(2,1)}, u32[]{:S(2)}, u32[]{:S(2)}) async-start(bf16[8,128,256]{2,1,0:T(8,128)(2,1)} %bitcast.58), calls=%async_computation | async-start | bytes 1048576 | tf_op jit(solution)/shard_map/all_to_all | solution.py:562
  139.9 3.5 %fusion = bf16[1,2048,256]{2,1,0:T(8,128)(2,1)} fusion(bf16[512,2048]{1,0:T(8,128)(2,1)} %bitcast.76, bf16[512,256]{1,0:T(8,128)(2,1)S(1)} %copy-done.27), kind=kOutput, calls=%fused_computation.4 | convolution fusion | flops 537395200 | bytes 3407872 | tf_op jit(solution)/shard_map/dot_general | solution.py:34
  143.5 1.8 fusion.1
  145.2 0.4 copy-done.25
  145.6 1.8 fusion.2
  147.3 0.7 copy.103
  148.0 28.4 %all-gather.11.cloned.1.call-done = bf16[512,1024]{1,0:T(8,128)(2,1)} async-done(((bf16[64,1024]{1,0:T(8,128)(2,1)}), bf16[512,1024]{1,0:T(8,128)(2,1)}) %all-gather.11.cloned.1.call-update) | async-done | bytes 1048592 | tf_op jit(solution)/shard_map/all_gather | solution.py:559
  176.4 1.2 copy-done.4
  177.7 3.9 %shard_map.230 = (bf16[128,1024]{1,0:T(8,128)(2,1)}, f32[128,64]{1,0:T(8,128)S(1)}, f32[128,16]{1,0:T(8,128)S(1)}) custom-call(bf16[128,1024]{1,0:T(8,128)(2,1)S(1)} %copy-done.2, bf16[128,64]{1,0:T(8,128)(2,1)S(1)} %copy.96.b_ref, f32[128,16]{1,0:T(8,128)S(1)} %copy.88.raw_ref, f32[128,16]{1,0:T(8,128)S(1)} %get-tuple-element.76.dt_ref, ...), custom_call_target="tpu_custom_call" | custom-call | flops 300000000 | bytes 4000000 | tf_op jit(solution)/shard_map/pallas_call | solution.py:567
  181.5 0.7 copy.102
  182.2 0.7 copy.104
  182.9 43.5 %all-gather.7.cloned.1.call-done = bf16[1024,1024]{1,0:T(8,128)(2,1)} async-done(((bf16[128,1024]{1,0:T(8,128)(2,1)}), bf16[1024,1024]{1,0:T(8,128)(2,1)}) %all-gather.7.cloned.1.call-update) | async-done | bytes 2097168 | tf_op jit(solution)/shard_map/all_gather | solution.py:528
  226.4 3.5 %fusion.24 = f32[256,1024]{1,0:T(8,128)} fusion(bf16[1024,256]{1,0:T(8,128)(2,1)} %bitcast.12, bf16[1024,1024]{1,0:T(8,128)(2,1)} %all-gather.7.cloned.1.call-done), kind=kOutput, calls=%fused_computation.39 | convolution fusion | flops 536870912 | bytes 3670016 | tf_op jit(solution)/shard_map/dot_general | solution.py:34
  (69 shorter events, 0.9 us)
Async XLA Ops:
  7.2 52.9 %copy-start = (bf16[1,2048,256]{2,1,0:T(8,128)(2,1)S(1)}, bf16[1,2048,256]{2,1,0:T(8,128)(2,1)}, u32[]{:S(2)}) copy-start(bf16[1,2048,256]{2,1,0:T(8,128)(2,1)} %param.20) | copy-start | bytes 3145732
  7.2 114.5 %all-gather.9.cloned.1.call-start = ((), (), s32[]{:S(2)}) async-start(), calls=%async_computation.2 | async-start | bytes 1179648 | tf_op jit(solution)/shard_map/all_gather | solution.py:510
  9.8 1.0 copy-start.1
  12.2 164.3 %all-gather.11.cloned.1.call-start = ((), (), s32[]{:S(2)}) async-start(), calls=%async_computation.3 | async-start | bytes 1179648 | tf_op jit(solution)/shard_map/all_gather | solution.py:559
  13.9 0.9 copy-start.5
  14.8 0.9 copy-start.9
  60.0 2.8 %copy-start.19 = (bf16[1,8,64,2048]{3,2,1,0:T(8,128)(2,1)}, bf16[1,8,64,2048]{3,2,1,0:T(8,128)(2,1)S(1)}, u32[]{:S(2)}) copy-start(bf16[1,8,64,2048]{3,2,1,0:T(8,128)(2,1)S(1)} %get-tuple-element.72) | copy-start | bytes 6291460
  60.1 2.8 %copy-start.15 = (bf16[1,8,64,2048]{3,2,1,0:T(8,128)(2,1)}, bf16[1,8,64,2048]{3,2,1,0:T(8,128)(2,1)S(1)}, u32[]{:S(2)}) copy-start(bf16[1,8,64,2048]{3,2,1,0:T(8,128)(2,1)S(1)} %get-tuple-element.71) | copy-start | bytes 6291460
  60.1 2.0 copy-start.21
  62.1 2.2 copy-start.22
  62.1 1.4 copy-start.33
  62.8 1.5 copy-start.24
  64.3 0.7 copy-start.26
  64.3 27.4 %copy-start.28 = (bf16[512,256]{1,0:T(8,128)(2,1)}, bf16[512,256]{1,0:T(8,128)(2,1)S(1)}, u32[]{:S(2)}) copy-start(bf16[512,256]{1,0:T(8,128)(2,1)S(1)} %get-tuple-element.73) | copy-start | bytes 786436
  65.0 2.7 %copy-start.32 = (bf16[128,64]{0,1:T(8,128)(2,1)S(1)}, bf16[128,64]{0,1:T(8,128)(2,1)}, u32[]{:S(2)}) copy-start(bf16[128,64]{0,1:T(8,128)(2,1)} %param.25) | copy-start | bytes 49156
  91.8 28.9 %copy-start.30 = (f32[8,1,16]{2,1,0:T(1,128)}, f32[8,1,16]{2,1,0:T(1,128)S(1)}, u32[]{:S(2)}) copy-start(f32[8,1,16]{2,1,0:T(1,128)S(1)} %all-gather.2) | copy-start | bytes 1540
  94.8 18.1 %copy-start.6 = (bf16[128,512]{1,0:T(8,128)(2,1)S(1)}, bf16[128,512]{1,0:T(8,128)(2,1)}, u32[]{:S(2)}) copy-start(bf16[128,512]{1,0:T(8,128)(2,1)} %cot_ref.3) | copy-start | bytes 393220
  94.8 26.1 %copy-start.18 = (bf16[2048,1024]{1,0:T(8,128)(2,1)S(1)}, bf16[2048,1024]{1,0:T(8,128)(2,1)}, u32[]{:S(2)}) copy-start(bf16[2048,1024]{1,0:T(8,128)(2,1)} %param.31) | copy-start | bytes 12582916
  120.7 0.9 copy-start.17
  120.9 1.0 copy-start.2
  120.9 1.0 copy-start.12
  120.9 1.0 copy-start.14
  121.9 1.2 copy-start.3
  123.1 0.9 copy-start.8
  126.4 0.7 copy-start.7
  130.2 0.6 copy-start.10
  130.8 8.9 %copy-start.31 = (f32[8,1,16]{2,1,0:T(1,128)S(1)}, f32[8,1,16]{2,1,0:T(1,128)}, u32[]{:S(2)}) copy-start(f32[8,1,16]{2,1,0:T(1,128)} %copy-done.30) | copy-start | bytes 1540
  130.8 9.1 %copy-start.27 = (bf16[512,256]{1,0:T(8,128)(2,1)S(1)}, bf16[512,256]{1,0:T(8,128)(2,1)}, u32[]{:S(2)}) copy-start(bf16[512,256]{1,0:T(8,128)(2,1)} %copy-done.26) | copy-start | bytes 786436
  130.9 95.6 %all-gather.7.cloned.1.call-start = ((), (), s32[]{:S(2)}) async-start(), calls=%async_computation.1 | async-start | bytes 2359296 | tf_op jit(solution)/shard_map/all_gather | solution.py:528
  133.5 49.4 %all-to-all-start = ((bf16[8,128,256]{2,1,0:T(8,128)(2,1)}), bf16[8,128,256]{2,1,0:T(8,128)(2,1)}, u32[]{:S(2)}, u32[]{:S(2)}) async-start(bf16[8,128,256]{2,1,0:T(8,128)(2,1)} %bitcast.58), calls=%async_computation | async-start | bytes 1048576 | tf_op jit(solution)/shard_map/all_to_all | solution.py:562
  139.9 3.5 %copy-start.20 = (bf16[1,8,64,2048]{3,2,1,0:T(8,128)(2,1)S(1)}, bf16[1,8,64,2048]{3,2,1,0:T(8,128)(2,1)}, u32[]{:S(2)}) copy-start(bf16[1,8,64,2048]{3,2,1,0:T(8,128)(2,1)} %copy-done.19) | copy-start | bytes 6291460
  139.9 3.5 %copy-start.29 = (bf16[512,256]{1,0:T(8,128)(2,1)S(1)}, bf16[512,256]{1,0:T(8,128)(2,1)}, u32[]{:S(2)}) copy-start(bf16[512,256]{1,0:T(8,128)(2,1)} %copy-done.28) | copy-start | bytes 786436
  143.4 1.8 copy-start.16
  143.4 1.8 copy-start.23
  143.5 2.1 copy-start.25
  145.6 1.8 copy-start.11
  145.6 30.9 %copy-start.13 = (f32[16]{0:T(128)S(1)}, f32[16]{0:T(128)}, u32[]{:S(2)}) copy-start(f32[16]{0:T(128)} %param.28) | copy-start | bytes 196
  176.4 1.2 copy-start.4
Sparse Core Ops, SparseCore 0:
  12.3 54.2 all-gather.8
  131.0 45.4 all-gather.10
  178.6 47.8 all-gather.6

commit v3 on v2

--- a/solution.py
+++ b/solution.py
@@ -11,6 +11,7 @@
 STATE = 64
 PAIR = 2 * HEAD_DIM
 EPS = 0.01
+EXTRA = 16
 HIGH = lax.Precision.HIGHEST
 F32 = jnp.float32
 BF16 = jnp.bfloat16
@@ -83,23 +84,50 @@
     run = run_ref[...]
     factor = dt_ref[...] * jnp.exp(run[-1:, :] - run)
     xe = silu(x_ref[...].astype(F32)) * wide(factor, table)
-    fresh_ref[...] = tn(silu(b_ref[...].astype(F32)), xe).astype(BF16)
+    fresh_ref[:STATE, :] = tn(silu(b_ref[...].astype(F32)), xe).astype(BF16)
+    rest = wide(jnp.broadcast_to(run[-1:, :], (EXTRA, run.shape[1])), table)
+    row = lax.broadcasted_iota(jnp.int32, rest.shape, 0)
+    extra = jnp.zeros_like(rest)
+    for k in range(3):
+        piece = rest.astype(BF16).astype(F32)
+        extra = jnp.where(row == k, piece, extra)
+        rest = rest - piece
+    fresh_ref[STATE:, :] = extra.astype(BF16)
 
 
 def weighted_sum(all_ref, weight_ref):
     def one(j, total):
-        return total + all_ref[j].astype(F32) * weight_ref[pl.ds(j, 1), :]
-
-    return lax.fori_loop(0, all_ref.shape[0], one, jnp.zeros(all_ref.shape[1:], F32))
+        return total + all_ref[j, :STATE, :].astype(F32) * weight_ref[pl.ds(j, 1), :]
+
+    return lax.fori_loop(0, all_ref.shape[0], one, jnp.zeros((STATE, all_ref.shape[2]), F32))
+
+
+def fill_carries(all_ref, ends_ref, fore_ref, back_ref):
+    count = all_ref.shape[0]
+    me = lax.axis_index("sp")
+
+    def one(j, _):
+        parts = all_ref[j, STATE:, :].astype(F32)
+        ends_ref[pl.ds(j, 1), :] = parts[0:1] + parts[1:2] + parts[2:3]
+        return 0
+
+    lax.fori_loop(0, count, one, 0)
+    j = lax.broadcasted_iota(jnp.int32, (count, count), 0)
+    i = lax.broadcasted_iota(jnp.int32, (count, count), 1)
+    own = lax.broadcasted_iota(jnp.int32, fore_ref.shape, 0)
+    ahead = ((i > j) & (i < me)).astype(F32)
+    behind = ((i < j) & (i > me)).astype(F32)
+    fore_ref[...] = jnp.where(own < me, jnp.exp(wide(ahead, ends_ref[...])), 0.0)
+    back_ref[...] = jnp.where(own > me, jnp.exp(wide(behind, ends_ref[...])), 0.0)
 
 
 def forward_kernel(
-    x_ref, b_ref, c_ref, z_ref, dt_ref, run_ref, run_t_ref, skip_ref, gain_ref, all_ref, coef_ref,
-    norm_ref, mixed_ref, state_ref, weight_ref,
+    x_ref, b_ref, c_ref, z_ref, dt_ref, run_ref, run_t_ref, skip_ref, gain_ref, all_ref,
+    norm_ref, mixed_ref, state_ref, back_ref, weight_ref, ends_ref,
 ):
     heads = dt_ref.shape[1]
     table = spread(heads)
-    weight_ref[...] = wide(coef_ref[...], table)
+    fill_carries(all_ref, ends_ref, weight_ref, back_ref)
     state = weighted_sum(all_ref, weight_ref)
     state_ref[...] = state
     x_act = silu(x_ref[...].astype(F32))
@@ -181,13 +209,12 @@
 def finish_kernel(
     x_ref, b_ref, raw_ref, dt_ref, run_ref, rate_ref, state_ref, all_ref, coef_ref, xs_grad_ref,
     x_grad_ref, run_grad_ref, b_grad_ref,
-    x_out_ref, b_out_ref, raw_out_ref, weight_ref,
+    x_out_ref, b_out_ref, raw_out_ref,
 ):
     heads = dt_ref.shape[1]
     rows = x_ref.shape[0]
     table = spread(heads)
-    weight_ref[...] = wide(coef_ref[...], table)
-    after = weighted_sum(all_ref, weight_ref)
+    after = weighted_sum(all_ref, coef_ref)
     x_act, x_slope = silu_and_slope(x_ref[...].astype(F32))
     b_act, b_slope = silu_and_slope(b_ref[...].astype(F32))
     dt = dt_ref[...]
@@ -477,18 +504,6 @@
     )(terms)
 
 
-def carries(last, axis):
-    count, me = lax.axis_size(axis), lax.axis_index(axis)
-    ends = lax.all_gather(last, axis)
-    j = jnp.arange(count)
-    i = j[None, :]
-    ahead = ((i > j[:, None]) & (i < me)).astype(F32)
-    behind = ((i < j[:, None]) & (i > me)).astype(F32)
-    fore = jnp.where((j < me)[:, None], jnp.exp(jnp.dot(ahead, ends, precision=HIGH)), 0.0)
-    back = jnp.where((j > me)[:, None], jnp.exp(jnp.dot(behind, ends, precision=HIGH)), 0.0)
-    return fore, back
-
-
 def body(
     moe_input, cotangent, expert_ids, routing_weights, gate_weight, up_weight, down_weight,
     inner_x, inner_b, inner_c, gate_z, step_raw, decay_rate, skip_weight, norm_gain, w_out,
@@ -506,9 +521,8 @@
     dt = jax.nn.softplus(step_raw)
     run = jnp.cumsum(-dt * rate, axis=0)
     run_t = run.T
-    (fresh,) = call(fresh_kernel, [((STATE, inner), BF16)], 40_000_000)(inner_x, inner_b, dt, run)
+    (fresh,) = call(fresh_kernel, [((STATE + EXTRA, inner), BF16)], 40_000_000)(inner_x, inner_b, dt, run)
     fresh_all = lax.all_gather(fresh, "sp")
-    fore, back = carries(run[-1], "sp")
 
     (sent,) = call(partial(dispatch_kernel, experts), [((2, slots, cols), BF16)], 200_000_000)(
         moe_input, cotangent, expert_ids, routing_weights
@@ -519,13 +533,12 @@
     routed_in, routed_grad = routed[0], routed[1]
 
     weight_rows = pltpu.VMEM((senders, inner), F32)
-    norm_rows, mixed, state = call(
+    norm_rows, mixed, state, back = call(
         forward_kernel,
-        [((rows, inner), BF16), ((rows, inner), F32), ((STATE, inner), F32)],
+        [((rows, inner), BF16), ((rows, inner), F32), ((STATE, inner), F32), ((senders, inner), F32)],
         300_000_000,
-        [weight_rows],
-    )(inner_x, inner_b, inner_c, gate_z, dt, run, run_t, skip, gain, fresh_all, fore)
-    norm_all = lax.all_gather(norm_rows, "sp", axis=0, tiled=True)
+        [weight_rows, weight_rows],
+    )(inner_x, inner_b, inner_c, gate_z, dt, run, run_t, skip, gain, fresh_all)
 
     gate_w, up_w, down_w = gate_weight[0], up_weight[0], down_weight[0]
     gate_pre = jnp.dot(routed_in, gate_w, preferred_element_type=F32)
@@ -537,12 +550,15 @@
     gate_grad = (hidden_grad * up_pre * sig * (1.0 + gate_pre * (1.0 - sig))).astype(BF16)
     up_grad = (hidden_grad * active).astype(BF16)
     terms = (nt(gate_grad, gate_w) + nt(up_grad, up_w)).astype(BF16)
+    terms, norm_rows = lax.optimization_barrier((terms, norm_rows))
+    norm_all = lax.all_gather(norm_rows, "sp", axis=0, tiled=True)
     returned = fold(terms.reshape(senders, slots // senders, tp * cols), tp).reshape(slots, cols)
     (mixer_cols,) = call(partial(combine_kernel, experts), [((rows, cols), BF16)], 100_000_000)(
         returned, cotangent, expert_ids
     )
     mixer_rows = lax.all_gather(mixer_cols, "tp", axis=1, tiled=True)
     norm_grad = jnp.dot(mixer_rows, w_out, preferred_element_type=F32)
+    norm_grad, norm_all = lax.optimization_barrier((norm_grad, norm_all))
     state_grad, xs_grad, x_grad, z_grad, run_grad, b_grad, c_grad = call(
         backward_kernel,
         [
@@ -568,7 +584,6 @@
         finish_kernel,
         [((rows, inner), BF16), ((rows, STATE), F32), ((rows, heads), F32)],
         300_000_000,
-        [weight_rows],
     )(
         inner_x, inner_b, step_raw, dt, run, rate, state, state_grads, back, xs_grad, x_grad,
         run_grad, b_grad,

time: 237 us -> 203 us (0.86)
  waiting for transfers between devices: 72.5 us -> 47.9 us
  blocking collectives: 31.1 us -> 7.73 us
  Pallas kernels: 73.2 us -> 84 us
  local copies, waits for them, and re-layouts: 18.7 us -> 28 us
  matrix products: 19.5 us -> 15 us
    all_gather x1 -> x0, blocking collectives: 23.9 us -> none  [carries(): ends = lax.all_gather(last, axis)]
    all_gather x1, waiting for transfers between devices: 43.5 us -> 23.8 us  [body(): norm_all = lax.all_gather(norm_rows, 'sp', axis=0, tiled=True)]
    all_gather x1, waiting for transfers between devices: 28.4 us -> 14.7 us  [body(): state_grads = lax.all_gather(state_grad, 'sp')]
    pallas_call x1, Pallas kernels: 18.1 us -> 28.4 us  [fold(): pl.pallas_call(partial(fold_kernel, count), out_shape=jax.ShapeDtypeStruc...]
    all_to_all x1, waiting for transfers between devices: 0.01 us -> 9.28 us  [body(): lax.all_to_all(mixer_blocks, 'sp', 0, 0, tiled=True)]
    unnamed x77 -> x104, local copies, waits for them, and re-layouts: 16.2 us -> 23.2 us
    dot_general x3, matrix products: 6.52 us -> 2.33 us  [nt(): lax.dot_general(a.astype(BF16), b.astype(BF16), (((1,), (1,)), ((), ())),...]
  transfers between devices with their start and end apart: 4 -> 4, of which waited for: 2 -> 3; matrix products, arithmetic and copies ran while one was open for 9% -> 11% of each run, Pallas kernels for 28% -> 36%
where the time goes in v3:
time: 203 us; the launch traced here: 202 us
  Pallas kernels  84 us (41%)
  waiting for transfers between devices  47.9 us (24%)
  local copies, waits for them, and re-layouts  28 us (14%)
  matrix products  15 us (7%)
  between operations  14.2 us (7%)
  blocking collectives  7.73 us (4%)
  starting transfers between devices  4.27 us (2%)
    pallas_call x1, Pallas kernels, route(): pl.pallas_call(partial(route_kernel, count), out_shape=jax.ShapeDtypeStru...  43.2 us
    pallas_call x1, Pallas kernels, fold(): pl.pallas_call(partial(fold_kernel, count), out_shape=jax.ShapeDtypeStruc...  28.4 us
    all_gather x1, waiting for transfers between devices, body(): norm_all = lax.all_gather(norm_rows, 'sp', axis=0, tiled=True)  23.8 us
    unnamed x104, local copies, waits for them, and re-layouts  23.2 us
    all_gather x1, waiting for transfers between devices, body(): state_grads = lax.all_gather(state_grad, 'sp')  14.7 us
    dot_general x4, matrix products, tn(): lax.dot_general(a.astype(BF16), b.astype(BF16), (((0,), (0,)), ((), ())),...  10.5 us
    all_to_all x1, waiting for transfers between devices, body(): lax.all_to_all(mixer_blocks, 'sp', 0, 0, tiled=True)  9.28 us
    all_gather x1, blocking collectives, body(): mixer_rows = lax.all_gather(mixer_cols, 'tp', axis=1, tiled=True)  7.73 us
  transfers between devices with their start and end apart: 4, of which 3 were waited for; matrix products, arithmetic and copies ran while one was open for 11% of the time, Pallas kernels for 36%

profile of v3, /device:TPU:0, one launch (start us, length us, event | category | flops | bytes accessed | tf_op | source)
XLA Modules:
  0.0 202.1 jit_solution(8983534967167035507)
XLA Ops:
  7.2 0.9 copy.74.b_ref
  8.2 0.8 copy.66.raw_ref
  9.0 0.7 negate_multiply_fusion
  9.9 0.9 copy-done.2
  10.8 1.5 shard_map.225
  12.4 0.8 copy.64.ids_ref
  13.2 0.8 copy.65.weight_ref
  14.1 0.9 copy-done.13
  15.0 0.9 copy-done.23
  15.9 1.1 shard_map.223
  17.0 43.2 %shard_map.224 = bf16[2,8,64,2048]{3,2,1,0:T(8,128)(2,1)S(1)} custom-call(bf16[2,8,64,512]{3,2,1,0:T(8,128)(2,1)S(1)} %bitcast.57), custom_call_target="tpu_custom_call" | custom-call | flops 10000000000 | bytes 8000000 | tf_op jit(solution)/shard_map/pallas_call | solution.py:380
  60.2 2.0 copy-done.1
  62.2 0.7 copy.75.c_ref
  62.9 2.7 %fusion.15 = (bf16[1,8,64,2048]{3,2,1,0:T(8,128)(2,1)S(1)}, bf16[1,8,64,2048]{3,2,1,0:T(8,128)(2,1)S(1)}) fusion(bf16[2,8,64,2048]{3,2,1,0:T(8,128)(2,1)} %copy-done.1), kind=kLoop, calls=%fused_computation.25 | loop fusion | bytes 8388608 | tf_op jit(solution)/shard_map/slice | solution.py:533
  65.7 0.7 fusion.5
  66.5 1.3 copy-done.37
  67.7 0.7 fusion.8
  69.1 0.8 multiply_convert_fusion.1
  70.0 0.7 fusion.3
  70.8 0.7 add_convert_fusion
  71.8 1.3 copy-done.4
  73.1 0.8 copy-done.11
  73.8 0.9 copy-done.15
  74.8 0.8 copy-done.21
  75.5 2.5 %shard_map.226 = (bf16[128,1024]{1,0:T(8,128)(2,1)S(1)}, f32[128,1024]{1,0:T(8,128)S(1)}, f32[64,1024]{1,0:T(8,128)S(1)}, f32[8,1024]{1,0:T(8,128)S(1)}) custom-call(bf16[128,1024]{1,0:T(8,128)(2,1)S(1)} %copy-done.3, bf16[128,64]{1,0:T(8,128)(2,1)S(1)} %copy-done.11, bf16[128,64]{1,0:T(8,128)(2,1)S(1)} %copy-done.21, bf16[128,1024]{1,0:T(8,128)(2,1)S(1)} %copy-done.15, ...), custom_call_target="tpu_custom_call" | custom-call | flops 300000000 | bytes 4000000 | tf_op jit(solution)/shard_map/pallas_call | solution.py:536
  78.0 0.7 copy-done.17
  78.7 0.7 copy-done.20
  80.1 0.8 copy-done.29
  81.0 28.4 %shard_map.227 = bf16[8,64,512]{2,1,0:T(8,128)(2,1)S(1)} custom-call(bf16[8,64,2048]{2,1,0:T(8,128)(2,1)S(1)} %bitcast.54), custom_call_target="tpu_custom_call" | custom-call | flops 10000000000 | bytes 4000000 | tf_op jit(solution)/shard_map/pallas_call | solution.py:488
  110.0 7.7 %all_gather.20 = bf16[128,2048]{1,0:T(8,128)(2,1)S(1)} all-gather(bf16[128,512]{1,0:T(8,128)(2,1)S(1)} %shard_map.228), channel_id=1, replica_groups=mesh['sp'=8,'tp'=4] {'tp'}, dimensions={1}, use_global_device_ids=true | all-gather | bytes 655360 | tf_op jit(solution)/shard_map/all_gather | solution.py:559
  117.8 0.7 fusion.16.up_ref
  118.5 23.8 %all-gather.6.cloned.1.call-done = bf16[1024,1024]{1,0:T(8,128)(2,1)} async-done(((bf16[128,1024]{1,0:T(8,128)(2,1)}), bf16[1024,1024]{1,0:T(8,128)(2,1)}) %all-gather.6.cloned.1.call-update) | async-done | bytes 2097168 | tf_op jit(solution)/shard_map/all_gather | solution.py:554
  142.3 0.9 copy-done.18
  143.2 1.0 copy-done.30
  144.3 3.1 %shard_map.229 = (bf16[64,1024]{1,0:T(8,128)(2,1)}, f32[128,1024]{1,0:T(8,128)S(1)}, f32[128,1024]{1,0:T(8,128)S(1)}, bf16[128,1024]{1,0:T(8,128)(2,1)}, f32[128...) custom-call(bf16[128,1024]{1,0:T(8,128)(2,1)S(1)} %copy-done.3, bf16[128,64]{1,0:T(8,128)(2,1)S(1)} %copy-done.12, ...), custom_call_target="tpu_custom_call" | custom-call | flops 600000000 | bytes 4000000 | tf_op jit(solution)/shard_map/pallas_call | solution.py:562
  147.4 2.0 copy.88
  149.4 4.1 %all-to-all-start = ((bf16[8,128,256]{2,1,0:T(8,128)(2,1)}), bf16[8,128,256]{2,1,0:T(8,128)(2,1)}, u32[]{:S(2)}, u32[]{:S(2)}) async-start(bf16[8,128,256]{2,1,0:T(8,128)(2,1)} %bitcast.53), calls=%async_computation | async-start | bytes 1048576 | tf_op jit(solution)/shard_map/all_to_all | solution.py:578
  153.6 3.5 %fusion = bf16[1,2048,256]{2,1,0:T(8,128)(2,1)} fusion(bf16[512,2048]{1,0:T(8,128)(2,1)} %bitcast.71, bf16[512,256]{1,0:T(8,128)(2,1)S(1)} %copy-done.43), kind=kOutput, calls=%fused_computation.4 | convolution fusion | flops 537395200 | bytes 3407872 | tf_op jit(solution)/shard_map/dot_general | solution.py:35
  157.1 1.8 fusion.1
  159.3 1.8 fusion.2
  161.0 0.7 copy.83
  161.7 9.3 %all-to-all-done = bf16[8,128,256]{2,1,0:T(8,128)(2,1)} async-done(((bf16[8,128,256]{2,1,0:T(8,128)(2,1)}), bf16[8,128,256]{2,1,0:T(8,128)(2,1)}, u32[]{:S(2)}, u32[]{:S(2)}) %all-to-all-start) | async-done | bytes 524320 | tf_op jit(solution)/shard_map/all_to_all | solution.py:578
  171.0 3.5 %fusion.17 = f32[256,1024]{1,0:T(8,128)} fusion(bf16[1024,256]{1,0:T(8,128)(2,1)} %bitcast.16, bf16[1024,1024]{1,0:T(8,128)(2,1)} %all-gather.6.cloned.1.call-done), kind=kOutput, calls=%fused_computation.27 | convolution fusion | flops 536870912 | bytes 3670016 | tf_op jit(solution)/shard_map/dot_general | solution.py:35
  174.5 14.7 %all-gather.10.cloned.1.call-done = bf16[512,1024]{1,0:T(8,128)(2,1)} async-done(((bf16[64,1024]{1,0:T(8,128)(2,1)}), bf16[512,1024]{1,0:T(8,128)(2,1)}) %all-gather.10.cloned.1.call-update) | async-done | bytes 1048592 | tf_op jit(solution)/shard_map/all_gather | solution.py:575
  189.2 1.2 copy-done.5
  190.4 3.7 %shard_map.230 = (bf16[128,1024]{1,0:T(8,128)(2,1)}, f32[128,64]{1,0:T(8,128)S(1)}, f32[128,16]{1,0:T(8,128)S(1)}) custom-call(bf16[128,1024]{1,0:T(8,128)(2,1)S(1)} %copy-done.3, bf16[128,64]{1,0:T(8,128)(2,1)S(1)} %copy-done.12, f32[128,16]{1,0:T(8,128)S(1)} %copy-done.7, f32[128,16]{1,0:T(8,128)S(1)} %get-tuple-element.77.dt_ref, ...), custom_call_target="tpu_custom_call" | custom-call | flops 300000000 | bytes 4000000 | tf_op jit(solution)/shard_map/pallas_call | solution.py:583
  194.2 0.7 copy.82
  194.9 0.7 copy.84
  (91 shorter events, 3.0 us)
Async XLA Ops:
  7.2 58.5 %copy-start = (bf16[1,2048,256]{2,1,0:T(8,128)(2,1)S(1)}, bf16[1,2048,256]{2,1,0:T(8,128)(2,1)}, u32[]{:S(2)}) copy-start(bf16[1,2048,256]{2,1,0:T(8,128)(2,1)} %param.20) | copy-start | bytes 3145732
  7.2 64.4 %all-gather.8.cloned.1.call-start = ((), (), s32[]{:S(2)}) async-start(), calls=%async_computation.2 | async-start | bytes 1474560 | tf_op jit(solution)/shard_map/all_gather | solution.py:525
  8.1 4.2 %copy-start.10 = (bf16[128,64]{1,0:T(8,128)(2,1)}, bf16[128,64]{1,0:T(8,128)(2,1)S(1)}, u32[]{:S(2)}) copy-start(bf16[128,64]{1,0:T(8,128)(2,1)S(1)} %copy.74.b_ref) | copy-start | bytes 49156
  9.0 51.2 %copy-start.6 = (f32[128,16]{1,0:T(8,128)}, f32[128,16]{1,0:T(8,128)S(1)}, u32[]{:S(2)}) copy-start(f32[128,16]{1,0:T(8,128)S(1)} %copy.66.raw_ref) | copy-start | bytes 24580
  9.9 1.0 copy-start.2
  12.3 130.0 %all-gather.6.cloned.1.call-start = ((), (), s32[]{:S(2)}) async-start(), calls=%async_computation.1 | async-start | bytes 2359296 | tf_op jit(solution)/shard_map/all_gather | solution.py:554
  13.2 47.0 %copy-start.8 = (s32[128,2]{1,0:T(8,128)}, s32[128,2]{1,0:T(8,128)S(1)}, u32[]{:S(2)}) copy-start(s32[128,2]{1,0:T(8,128)S(1)} %copy.64.ids_ref) | copy-start | bytes 3076
  14.0 0.9 copy-start.13
  15.0 0.9 copy-start.23
  17.0 45.3 %copy-start.46 = (bf16[128,64]{0,1:T(8,128)(2,1)S(1)}, bf16[128,64]{0,1:T(8,128)(2,1)}, u32[]{:S(2)}) copy-start(bf16[128,64]{0,1:T(8,128)(2,1)} %param.25) | copy-start | bytes 49156
  60.2 2.0 copy-start.1
  65.7 2.8 %copy-start.35 = (bf16[1,8,64,2048]{3,2,1,0:T(8,128)(2,1)}, bf16[1,8,64,2048]{3,2,1,0:T(8,128)(2,1)S(1)}, u32[]{:S(2)}) copy-start(bf16[1,8,64,2048]{3,2,1,0:T(8,128)(2,1)S(1)} %get-tuple-element.73) | copy-start | bytes 6291460
  65.7 2.8 %copy-start.31 = (bf16[1,8,64,2048]{3,2,1,0:T(8,128)(2,1)}, bf16[1,8,64,2048]{3,2,1,0:T(8,128)(2,1)S(1)}, u32[]{:S(2)}) copy-start(bf16[1,8,64,2048]{3,2,1,0:T(8,128)(2,1)S(1)} %get-tuple-element.72) | copy-start | bytes 6291460
  65.7 2.0 %copy-start.37 = (bf16[1,2048,256]{2,1,0:T(8,128)(2,1)S(1)}, bf16[1,2048,256]{2,1,0:T(8,128)(2,1)}, u32[]{:S(2)}) copy-start(bf16[1,2048,256]{2,1,0:T(8,128)(2,1)} %param.21) | copy-start | bytes 3145732
  67.7 2.3 %copy-start.38 = (f32[512,256]{1,0:T(8,128)}, f32[512,256]{1,0:T(8,128)S(1)}, u32[]{:S(2)}) copy-start(f32[512,256]{1,0:T(8,128)S(1)} %fusion.5) | copy-start | bytes 1572868
  67.7 1.4 copy-start.47
  68.5 1.5 copy-start.40
  70.0 0.8 copy-start.42
  70.0 0.8 copy-start.44
  70.8 0.9 copy-start.3
  70.8 0.9 copy-start.26
  70.8 0.9 copy-start.28
  71.8 1.3 copy-start.4
  73.1 0.8 copy-start.11
  73.8 0.9 copy-start.15
  80.1 0.8 copy-start.29
  80.9 108.3 %all-gather.10.cloned.1.call-start = ((), (), s32[]{:S(2)}) async-start(), calls=%async_computation.3 | async-start | bytes 1179648 | tf_op jit(solution)/shard_map/all_gather | solution.py:575
  80.9 28.5 %copy-start.9 = (s32[128,2]{1,0:T(8,128)S(1)}, s32[128,2]{1,0:T(8,128)}, u32[]{:S(2)}) copy-start(s32[128,2]{1,0:T(8,128)} %copy-done.8) | copy-start | bytes 3076
  80.9 28.5 %copy-start.14 = (bf16[128,512]{1,0:T(8,128)(2,1)S(1)}, bf16[128,512]{1,0:T(8,128)(2,1)}, u32[]{:S(2)}) copy-start(bf16[128,512]{1,0:T(8,128)(2,1)} %cot_ref.3) | copy-start | bytes 393220
  80.9 36.8 %copy-start.34 = (bf16[2048,1024]{1,0:T(8,128)(2,1)S(1)}, bf16[2048,1024]{1,0:T(8,128)(2,1)}, u32[]{:S(2)}) copy-start(bf16[2048,1024]{1,0:T(8,128)(2,1)} %param.31) | copy-start | bytes 12582916
  117.8 24.5 %copy-start.33 = (bf16[128,2048]{1,0:T(8,128)(2,1)}, bf16[128,2048]{1,0:T(8,128)(2,1)S(1)}, u32[]{:S(2)}) copy-start(bf16[128,2048]{1,0:T(8,128)(2,1)S(1)} %all_gather.20) | copy-start | bytes 1572868
  117.8 24.5 %copy-start.12 = (bf16[128,64]{1,0:T(8,128)(2,1)S(1)}, bf16[128,64]{1,0:T(8,128)(2,1)}, u32[]{:S(2)}) copy-start(bf16[128,64]{1,0:T(8,128)(2,1)} %copy-done.10) | copy-start | bytes 49156
  117.8 24.5 %copy-start.16 = (bf16[128,1024]{1,0:T(8,128)(2,1)S(1)}, bf16[128,1024]{1,0:T(8,128)(2,1)}, u32[]{:S(2)}) copy-start(bf16[128,1024]{1,0:T(8,128)(2,1)} %z_ref.3) | copy-start | bytes 786436
  117.8 24.5 %copy-start.22 = (bf16[128,64]{1,0:T(8,128)(2,1)S(1)}, bf16[128,64]{1,0:T(8,128)(2,1)}, u32[]{:S(2)}) copy-start(bf16[128,64]{1,0:T(8,128)(2,1)} %copy.75.c_ref) | copy-start | bytes 49156
  142.3 1.0 copy-start.18
  143.2 1.0 copy-start.30
  147.4 6.2 %copy-start.43 = (bf16[512,256]{1,0:T(8,128)(2,1)S(1)}, bf16[512,256]{1,0:T(8,128)(2,1)}, u32[]{:S(2)}) copy-start(bf16[512,256]{1,0:T(8,128)(2,1)} %copy-done.42) | copy-start | bytes 786436
  149.4 21.6 %all-to-all-start = ((bf16[8,128,256]{2,1,0:T(8,128)(2,1)}), bf16[8,128,256]{2,1,0:T(8,128)(2,1)}, u32[]{:S(2)}, u32[]{:S(2)}) async-start(bf16[8,128,256]{2,1,0:T(8,128)(2,1)} %bitcast.53), calls=%async_computation | async-start | bytes 1048576 | tf_op jit(solution)/shard_map/all_to_all | solution.py:578
  153.6 3.5 %copy-start.36 = (bf16[1,8,64,2048]{3,2,1,0:T(8,128)(2,1)S(1)}, bf16[1,8,64,2048]{3,2,1,0:T(8,128)(2,1)}, u32[]{:S(2)}) copy-start(bf16[1,8,64,2048]{3,2,1,0:T(8,128)(2,1)} %copy-done.35) | copy-start | bytes 6291460
  153.6 3.5 %copy-start.45 = (bf16[512,256]{1,0:T(8,128)(2,1)S(1)}, bf16[512,256]{1,0:T(8,128)(2,1)}, u32[]{:S(2)}) copy-start(bf16[512,256]{1,0:T(8,128)(2,1)} %copy-done.44) | copy-start | bytes 786436
  157.1 1.8 copy-start.32
  157.1 1.8 copy-start.39
  157.1 2.1 %copy-start.41 = (f32[512,256]{1,0:T(8,128)S(1)}, f32[512,256]{1,0:T(8,128)}, u32[]{:S(2)}) copy-start(f32[512,256]{1,0:T(8,128)} %copy-done.40) | copy-start | bytes 1572868
  161.0 28.2 %copy-start.7 = (f32[128,16]{1,0:T(8,128)S(1)}, f32[128,16]{1,0:T(8,128)}, u32[]{:S(2)}) copy-start(f32[128,16]{1,0:T(8,128)} %copy-done.6) | copy-start | bytes 24580
  161.0 28.2 %copy-start.19 = (f32[64,1024]{1,0:T(8,128)S(1)}, f32[64,1024]{1,0:T(8,128)}, u32[]{:S(2)}) copy-start(f32[64,1024]{1,0:T(8,128)} %copy-done.17) | copy-start | bytes 786436
  161.0 28.2 %copy-start.25 = (f32[8,1024]{1,0:T(8,128)S(1)}, f32[8,1024]{1,0:T(8,128)}, u32[]{:S(2)}) copy-start(f32[8,1024]{1,0:T(8,128)} %copy-done.24) | copy-start | bytes 98308
  161.0 28.2 %copy-start.27 = (f32[16]{0:T(128)S(1)}, f32[16]{0:T(128)}, u32[]{:S(2)}) copy-start(f32[16]{0:T(128)} %param.28) | copy-start | bytes 196
  189.2 1.2 copy-start.5
  (4 other events, 2.8 us)
Sparse Core Ops, SparseCore 0:
  12.4 56.4 all-gather.7
  81.0 61.2 all-gather.5
  147.5 41.6 all-gather.9
